TPU v7x, 32 devices: a whole 2x2x4 slice. The times are simulated.
32 devices in a mesh: ep: 8 (over z, y), tp: 4 (over x, core).
Axes of the slice: x: 2, y: 2, z: 4, core: 2. Of those that a mesh axis runs over, the one named last changes fastest.
Arguments:
- hidden: bfloat16 [512, 2048], P('ep'), may hold values from -10 to 10
- mix_gain: bfloat16 [2048], replicated, may hold values from 0.099609375 to 1.8984375
- proj_x: bfloat16 [2048, 2048], P('ep', 'tp'), may hold values from -0.125 to 0.125
- proj_y: bfloat16 [2048, 2048], P('ep', 'tp'), may hold values from -0.125 to 0.125
- conv_taps: bfloat16 [4, 2048], P(None, 'tp'), may hold values from -3 to 3
- input_gate: bfloat16 [32, 64, 64], P('tp'), may hold values from -0.75 to 0.75
- decay_gate: bfloat16 [32, 64, 64], P('tp'), may hold values from -0.75 to 0.75
- decay_param: float32 [2048], P('tp'), may hold values from 1 to 6
- proj_out: bfloat16 [2048, 2048], P('tp'), may hold values from -0.125 to 0.125
- conv_state: bfloat16 [512, 3, 2048], P('ep', None, 'tp'), may hold values from -6 to 6
- lru_state: float32 [512, 2048], P('ep', 'tp'), may hold values from -6 to 6
- ffn_gain: bfloat16 [2048], replicated, may hold values from 0.099609375 to 1.8984375
- routes: int32 [512, 2], P('ep'), may hold values from 0 to 7, all different within a row; in each aligned block of 64 rows (0 to 63, 64 to 127, ...) at most 18 rows name the same one
- route_weights: float32 [512, 2], P('ep'), may hold values from 0.2 to 1
- expert_gate: bfloat16 [8, 2048, 3072], P('ep', None, 'tp'), may hold values from -0.125 to 0.125
- expert_up: bfloat16 [8, 2048, 3072], P('ep', None, 'tp'), may hold values from -0.125 to 0.125
- expert_down: bfloat16 [8, 3072, 2048], P('ep', 'tp'), may hold values from -0.109375 to 0.109375
- dense_gate: bfloat16 [2048, 6144], P('tp', 'ep'), may hold values from -0.125 to 0.125
- dense_up: bfloat16 [2048, 6144], P('tp', 'ep'), may hold values from -0.125 to 0.125
- dense_down: bfloat16 [6144, 2048], P('ep', 'tp'), may hold values from -0.078125 to 0.078125
- branch_gate: float32 [2048], P('tp'), may hold values from -4 to 4
Outputs:
- new_hidden: bfloat16 [512, 2048], P('ep', 'tp')
- new_lru: float32 [512, 2048], P('ep', 'tp')
- new_conv: bfloat16 [512, 3, 2048], P('ep', None, 'tp')
Inputs may be any that keep to these rules, and one draw needn't show every extreme that they name: `routes`: each row names 2 different experts. In the 64 rows of one index of ep, no expert is named by more than 18 rows, a bound that some block reaches.
All inputs are finite; a program needn't handle non-finite values.
Results may differ from a plain program's by a relative error of at most 0.017.
Values may be sent and summed in bfloat16 or wider, within the bound.
A program may use at most 128 MiB of HBM per device.

v0:
```python
import functools

import jax
import jax.numpy as jnp
from jax import lax
from jax.experimental import pallas as pl
from jax.experimental.pallas import tpu as pltpu
from jax.sharding import PartitionSpec as P

epsilon = 1e-06
decay_scale = 8.0
MESH = pl.DeviceIdType.MESH
F32 = jnp.float32
BF16 = jnp.bfloat16


def dot(a, b):
    return jnp.dot(a, b, preferred_element_type=F32)


def layer_kernel(
    E, T, slots,
    hidden, mix_gain, routes, weights, conv_old, taps, ig, dgate, decay_param, lru, ffn_gain, branch,
    wx_h, wy_h, dg_h, du_h, po_h, eg_h, eu_h, ed_h, dd_h,
    new_hidden, new_lru, x_out,
    ct, w_ref, bd, wx, wy, dg, du, po, eg, eu, ed, dd, nb, dwp, dwr, spread, pm, pacc, yrec, zout, zrec, ctr, acc,
    mbuf, mrec, qbuf, qrec, xall, hacc, aall, xe, hid, sel, ebuf, erec, dtmp, om, dacc, orm, oz, ozr,
    summed_ref,
    load_sem, nb_s, nb_r, ct_s, ct_r, pm_s, pm_r, pz_s, pz_r, dw_s, dw_r, mx_s, mx_r, q_s, q_r,
    xr_s, xm_s, x2_s, x1_s, x_r, a_s, a_r, er_s, er_r, om_s, om_r, oz_s, oz_r,
):
    e = lax.axis_index("ep")
    t = lax.axis_index("tp")
    M, D = hidden.shape
    C = D // T
    R = wx.shape[0]
    G = E // 2
    g0 = e // 2
    par = lax.rem(e, 2)
    mate = e + 1 - 2 * par
    own_cols = pl.ds(pl.multiple_of(t * C, 128), C)

    def ep_peer(k):
        return lax.rem(e + k, E)

    def ep_from(k):
        return lax.rem(e + E - k, E)

    def group(k):
        return lax.rem(g0 + k, G)

    def rail_from(k):
        return 2 * lax.rem(g0 + G - k, G) + par

    def mate_of(s):
        return s + 1 - 2 * lax.rem(s, 2)

    def tp_peer(k):
        return lax.rem(t + k, T)

    across = lax.rem(t + T // 2, T)
    beside = t + 1 - 2 * lax.rem(t, 2)
    diagonal = lax.rem(beside + T // 2, T)

    loads = [
        pltpu.make_async_copy(src, dst, load_sem.at[i])
        for i, (src, dst) in enumerate(
            ((po_h, po), (eg_h, eg), (eu_h, eu), (ed_h, ed), (dd_h, dd),
             (wx_h, wx), (wy_h, wy), (dg_h, dg), (du_h, du))
        )
    ]
    own_dw = pltpu.make_async_copy(dwp.at[t], dwr.at[t], load_sem.at[9])
    for i in (5, 6, 7, 8, 0):
        loads[i].start()

    def rcopy(src, dst, s, r, ep=None, tp=None):
        return pltpu.make_async_remote_copy(
            src_ref=src, dst_ref=dst, send_sem=s, recv_sem=r,
            device_id=(e if ep is None else ep, t if tp is None else tp),
            device_id_type=MESH,
        )

    barrier = pltpu.get_barrier_semaphore()

    @pl.loop(1, E)
    def _(k):
        pl.semaphore_signal(barrier, inc=1, device_id=(ep_peer(k), t), device_id_type=MESH)

    for k in range(1, T):
        pl.semaphore_signal(barrier, inc=1, device_id=(e, tp_peer(k)), device_id_type=MESH)
    hf = hidden[...].astype(F32)
    inv = lax.rsqrt(jnp.mean(hf * hf, axis=-1, keepdims=True) + epsilon)
    normed = (hf * inv * mix_gain[...].astype(F32)).astype(BF16)
    for p in range(E):
        nb[p] = normed[:, p * R:(p + 1) * R]
    for p in range(E):
        ct[p] = jnp.sum(jnp.where(routes[...] == p, weights[...], 0.0), axis=0, keepdims=True)
    pl.semaphore_wait(barrier, E - 1 + T - 1)

    @pl.loop(1, E)
    def _(k):
        p = ep_peer(k)
        rcopy(nb.at[p], spread.at[e], nb_s.at[p], nb_r.at[e], ep=p).start()
        rcopy(ct.at[p], ctr.at[e], ct_s.at[p], ct_r.at[e], ep=p).start()

    loads[7].wait()
    loads[8].wait()
    h = dg.shape[1] // T
    half = dwp.shape[2] // 2
    if half != h:
        dwp[...] = jnp.zeros_like(dwp)
    for j in range(T):
        dwp[j, :, :h] = dg[:, j * h:(j + 1) * h]
        dwp[j, :, half:half + h] = du[:, j * h:(j + 1) * h]
    own_dw.start()
    for k in range(1, T):
        j = tp_peer(k)
        rcopy(dwp.at[j], dwr.at[t], dw_s.at[j], dw_r.at[t], tp=j).start()
    for l in loads[1:5]:
        l.start()

    spread[e] = nb[e]
    loads[5].wait()
    loads[6].wait()

    def arrive(s):
        rcopy(nb.at[s], spread.at[s], nb_s.at[s], nb_r.at[s], ep=s).wait_recv()

    def share(g):
        blk = spread[2 * g + 1 - par]
        pm[g, :, :C] = dot(blk, wx[...]).astype(BF16)
        pm[g, :, C:] = dot(blk, wy[...]).astype(BF16)
        rcopy(pm.at[g], yrec.at[g], pm_s.at[g], pm_r.at[g], ep=mate).start()
        blk = spread[2 * g + par]
        pacc[g, :, :C] = dot(blk, wx[...])
        pacc[g, :, C:] = dot(blk, wy[...])

    def pass_on(g):
        rcopy(pm.at[g], yrec.at[g], pm_s.at[g], pm_r.at[g], ep=mate).wait_recv()
        zout[g] = (pacc[g] + yrec[g].astype(F32)).astype(BF16)
        rcopy(zout.at[g], zrec.at[g0], pz_s.at[g], pz_r.at[g0], ep=2 * g + par).start()

    @pl.loop(1, G)
    def _(k):
        g = group(k)
        arrive(2 * g + 1 - par)
        arrive(2 * g + par)
        share(g)

        @pl.when(k > 1)
        def _():
            pass_on(group(k - 1))

    arrive(mate)
    share(g0)
    pass_on(group(G - 1))

    @pl.loop(1, E)
    def _(k):
        s = ep_from(k)
        rcopy(ct.at[s], ctr.at[s], ct_s.at[s], ct_r.at[s], ep=s).wait_recv()

    ctr[e] = ct[e]
    N = E * M
    for s in range(E):
        w_ref[:, s * M:(s + 1) * M] = ctr[s]
    w_row = w_ref[...]
    bd[...] = jnp.zeros_like(bd)
    block = ig.shape[1]
    width = bd.shape[1]
    per = width // block
    for i in range(ig.shape[0]):
        lo = i % per * block
        bd[i // per, lo:lo + block, lo:lo + block] = ig[i]
        bd[i // per, lo:lo + block, width + lo:width + lo + block] = dgate[i]
    nblk = min(N, 512)
    tri = (
        lax.broadcasted_iota(jnp.int32, (nblk, nblk), 0)
        < lax.broadcasted_iota(jnp.int32, (nblk, nblk), 1)
    ).astype(F32).astype(BF16)
    base = jnp.zeros((1, 1), F32)
    w_slot = jnp.zeros((slots, 1), F32)
    for b in range(N // nblk):
        w_b = w_row[:, b * nblk:(b + 1) * nblk]
        m_b = (w_b > 0.0).astype(F32)
        rank = dot(jnp.broadcast_to(m_b, (16, nblk)).astype(BF16), tri)[0:1, :] + base
        base = base + jnp.sum(m_b, axis=1, keepdims=True)
        hit = (
            lax.broadcasted_iota(jnp.int32, (slots, nblk), 0).astype(F32) == rank
        ).astype(F32) * m_b
        sel[:, b * nblk:(b + 1) * nblk] = hit.astype(BF16)
        w_slot = w_slot + jnp.sum(hit * w_b, axis=1, keepdims=True)

    rcopy(pm.at[g0], yrec.at[g0], pm_s.at[g0], pm_r.at[g0], ep=mate).wait_recv()
    acc[...] = pacc[g0] + yrec[g0].astype(F32)

    @pl.loop(1, G)
    def _(k):
        g = group(k)
        rcopy(zout.at[g], zrec.at[g], pz_s.at[g], pz_r.at[g], ep=2 * g + par).wait_recv()
        acc[...] += zrec[g].astype(F32)

    x_b = acc[:, :C].astype(BF16)
    y_b = acc[:, C:].astype(BF16)
    x_out[...] = x_b
    conv_pre = conv_old[0].astype(F32) * taps[0:1, :].astype(F32)
    for i in range(1, taps.shape[0] - 1):
        conv_pre = conv_pre + conv_old[i].astype(F32) * taps[i:i + 1, :].astype(F32)
    conv = (conv_pre + x_b.astype(F32) * taps[taps.shape[0] - 1:, :].astype(F32)).astype(BF16)
    gi, gd = [], []
    for i in range(C // width):
        g = dot(conv[:, i * width:(i + 1) * width], bd[i])
        gi.append(g[:, :width])
        gd.append(g[:, width:])
    gate_in = jax.nn.sigmoid(jnp.concatenate(gi, axis=1))
    gate_dec = jax.nn.sigmoid(jnp.concatenate(gd, axis=1))
    dp = decay_param[...]
    log_decay = decay_scale * gate_dec * (jnp.minimum(dp, 0.0) - jnp.log1p(jnp.exp(-jnp.abs(dp))))
    decay = jnp.exp(log_decay)
    inject = jnp.sqrt(-jnp.tanh(log_decay) * (1.0 + decay * decay))
    state = decay * lru[...] + inject * gate_in * conv.astype(F32)
    new_lru[...] = state
    gated = (state * jax.nn.gelu(y_b.astype(F32), approximate=True)).astype(BF16)

    loads[0].wait()
    order = [tp_peer(k) for k in (2, 3, 1)] if T == 4 else [tp_peer(k) for k in range(1, T)]
    for j in order:
        cols = pl.ds(pl.multiple_of(j * C, 128), C)
        mbuf[j] = dot(gated, po[:, cols]).astype(BF16)
        rcopy(mbuf.at[j], mrec.at[t], mx_s.at[j], mx_r.at[t], tp=j).start()
    mixer = dot(gated, po[:, own_cols]).astype(BF16).astype(F32)
    for j in reversed(order):
        rcopy(mbuf.at[j], mrec.at[j], mx_s.at[j], mx_r.at[j], tp=j).wait_recv()
        mixer = mixer + mrec[j].astype(F32)
    summed = (hidden[:, own_cols].astype(F32) + mixer).astype(BF16)
    summed_ref[...] = summed
    sf = summed.astype(F32)
    ssq = jnp.sum(sf * sf, axis=1, keepdims=True)
    qbuf[...] = jnp.broadcast_to(ssq, qbuf.shape)
    for j in order:
        rcopy(qbuf, qrec.at[t], q_s.at[j], q_r.at[t], tp=j).start()
    total = qbuf[...]
    for j in reversed(order):
        rcopy(qbuf, qrec.at[j], q_s.at[j], q_r.at[j], tp=j).wait_recv()
        total = total + qrec[j]
    scale = lax.rsqrt(total[:, 0:1] * (1.0 / D) + epsilon)
    xall[t, e] = (sf * scale * ffn_gain[:, own_cols].astype(F32)).astype(BF16)

    def to_mate(s):
        rcopy(xall.at[t, s], xall.at[t, s], xm_s.at[s], x_r.at[t, s], ep=mate).start()

    @pl.loop(1, G)
    def _(k):
        g = group(k)
        rcopy(xall.at[t, e], xall.at[t, e], xr_s.at[g], x_r.at[t, e], ep=2 * g + par).start()

    to_mate(e)

    def spread_tp(s):
        rcopy(xall.at[t, s], xall.at[t, s], x2_s.at[s], x_r.at[t, s], tp=across).start()
        rcopy(xall.at[t, s], xall.at[t, s], x1_s.at[0, s], x_r.at[t, s], tp=beside).start()

    def forward(s):
        rcopy(xall.at[across, s], xall.at[across, s], x2_s.at[s], x_r.at[across, s], tp=across).wait_recv()
        rcopy(xall.at[across, s], xall.at[across, s], x1_s.at[1, s], x_r.at[across, s], tp=beside).start()

    def arrived(s, p):
        rcopy(xall.at[t, s], xall.at[t, s], xm_s.at[s], x_r.at[t, s], ep=p).wait_recv()

    spread_tp(e)

    @pl.loop(1, G)
    def _(k):
        s = rail_from(k)
        arrived(s, s)
        to_mate(s)
        spread_tp(s)
        last = mate_of(rail_from(k - 1))
        arrived(last, mate)
        spread_tp(last)
        forward(rail_from(k - 1))

        @pl.when(k > 1)
        def _():
            forward(mate_of(rail_from(k - 2)))

    last = mate_of(rail_from(G - 1))
    arrived(last, mate)
    spread_tp(last)
    forward(rail_from(G - 1))
    if G > 1:
        forward(mate_of(rail_from(G - 2)))
    forward(last)

    @pl.loop(0, E)
    def _(s):
        rcopy(xall.at[beside, s], xall.at[beside, s], x1_s.at[0, s], x_r.at[beside, s], tp=beside).wait_recv()
        rcopy(xall.at[diagonal, s], xall.at[diagonal, s], x1_s.at[1, s], x_r.at[diagonal, s], tp=beside).wait_recv()

    own_dw.wait()
    for j in order:
        rcopy(dwp.at[j], dwr.at[j], dw_s.at[j], dw_r.at[j], tp=j).wait_recv()
    rows = min(N, 512)

    @pl.loop(0, N // rows)
    def _(b):
        hacc[...] = jnp.zeros_like(hacc)
        eb = rows // M

        @pl.loop(0, T)
        def _(q):
            xq = xall[q, pl.ds(b * eb, eb)].reshape(rows, C)
            hacc[...] += dot(xq, dwr[q])

        h = hacc[...]
        half = h.shape[1] // 2
        act = jax.nn.silu(h) * pltpu.roll(h, half, axis=1)
        aall[t, pl.ds(pl.multiple_of(b * rows, 16), rows), :] = act[:, :half].astype(BF16)

    a_across = rcopy(aall.at[t], aall.at[t], a_s.at[0], a_r.at[t], tp=across)
    a_beside = rcopy(aall.at[t], aall.at[t], a_s.at[1], a_r.at[t], tp=beside)
    a_across.start()
    a_beside.start()

    @pl.loop(0, T)
    def _(q):
        cols = pl.ds(pl.multiple_of(q * C, 128), C)
        xe[:, cols] = dot(sel[...], xall[q].reshape(N, C)).astype(BF16)

    loads[1].wait()
    loads[2].wait()
    FH = eg.shape[1]
    nch = 256 if FH % 256 == 0 else FH

    @pl.loop(0, FH // nch)
    def _(n):
        cols = pl.ds(pl.multiple_of(n * nch, 128), nch)
        g = dot(xe[...], eg[:, cols])
        u = dot(xe[...], eu[:, cols])
        hid[:, cols] = (jax.nn.silu(g) * u).astype(BF16)

    a_in = rcopy(aall.at[across], aall.at[across], a_s.at[0], a_r.at[across], tp=across)
    a_in.wait_recv()
    a_fwd = rcopy(aall.at[across], aall.at[across], a_s.at[2], a_r.at[across], tp=beside)
    a_fwd.start()

    loads[3].wait()
    for j in order:
        cols = pl.ds(pl.multiple_of(j * C, 128), C)
        ebuf[j] = dot(hid[...], ed[:, cols]).astype(BF16)
        rcopy(ebuf.at[j], erec.at[t], er_s.at[j], er_r.at[t], tp=j).start()
    ebuf[t] = dot(hid[...], ed[:, own_cols]).astype(BF16)

    loads[4].wait()
    rcopy(aall.at[beside], aall.at[beside], a_s.at[1], a_r.at[beside], tp=beside).wait_recv()
    rcopy(aall.at[diagonal], aall.at[diagonal], a_s.at[2], a_r.at[diagonal], tp=beside).wait_recv()
    red = ebuf[t].astype(F32)
    for j in reversed(order):
        rcopy(ebuf.at[j], erec.at[j], er_s.at[j], er_r.at[j], tp=j).wait_recv()
        red = red + erec[j].astype(F32)
    red = (red.astype(BF16).astype(F32) * w_slot).astype(BF16)
    gate = jax.nn.sigmoid(branch[...])
    ebuf[t] = red
    pair = 2 * M

    def block(g):
        rws = pl.ds(pl.multiple_of(g * pair, 128 if pair % 128 == 0 else 16), pair)
        d = dot(aall[0, rws, :], dd[0])
        for q in range(1, T):
            d = d + dot(aall[q, rws, :], dd[q])
        d = d * gate + lax.dot_general(
            sel[:, rws], ebuf[t], (((0,), (0,)), ((), ())), preferred_element_type=F32
        )
        dtmp[...] = d.reshape(2, M, C)
        om[g] = dtmp[1 - par].astype(BF16)
        rcopy(om.at[g], orm.at[g], om_s.at[g], om_r.at[g], ep=mate).start()
        dacc[g] = dtmp[par]

    def block_on(g):
        rcopy(om.at[g], orm.at[g], om_s.at[g], om_r.at[g], ep=mate).wait_recv()
        oz[g] = (dacc[g] + orm[g].astype(F32)).astype(BF16)
        rcopy(oz.at[g], ozr.at[g0], oz_s.at[g], oz_r.at[g0], ep=2 * g + par).start()

    @pl.loop(1, G)
    def _(k):
        block(group(k))

        @pl.when(k > 1)
        def _():
            block_on(group(k - 1))

    block(g0)
    block_on(group(G - 1))
    rcopy(om.at[g0], orm.at[g0], om_s.at[g0], om_r.at[g0], ep=mate).wait_recv()
    acc[:, :C] = summed_ref[...].astype(F32) + dacc[g0] + orm[g0].astype(F32)

    @pl.loop(1, G)
    def _(k):
        g = group(k)
        rcopy(oz.at[g], ozr.at[g], oz_s.at[g], oz_r.at[g], ep=2 * g + par).wait_recv()
        acc[:, :C] += ozr[g].astype(F32)

    new_hidden[...] = acc[:, :C].astype(BF16)

    @pl.loop(1, E)
    def _(k):
        p = ep_peer(k)
        rcopy(nb.at[p], spread.at[e], nb_s.at[p], nb_r.at[e], ep=p).wait_send()
        rcopy(ct.at[p], ctr.at[e], ct_s.at[p], ct_r.at[e], ep=p).wait_send()

    @pl.loop(0, G)
    def _(g):
        rcopy(pm.at[g], yrec.at[g], pm_s.at[g], pm_r.at[g], ep=mate).wait_send()
        rcopy(om.at[g], orm.at[g], om_s.at[g], om_r.at[g], ep=mate).wait_send()
        s = 2 * g + par
        rcopy(xall.at[t, s], xall.at[t, s], xm_s.at[s], x_r.at[t, s], ep=mate).wait_send()

    @pl.loop(1, G)
    def _(k):
        g = group(k)
        p = 2 * g + par
        rcopy(zout.at[g], zrec.at[g0], pz_s.at[g], pz_r.at[g0], ep=p).wait_send()
        rcopy(oz.at[g], ozr.at[g0], oz_s.at[g], oz_r.at[g0], ep=p).wait_send()
        rcopy(xall.at[t, e], xall.at[t, e], xr_s.at[g], x_r.at[t, e], ep=p).wait_send()

    for j in order:
        rcopy(dwp.at[j], dwr.at[t], dw_s.at[j], dw_r.at[t], tp=j).wait_send()
        rcopy(mbuf.at[j], mrec.at[t], mx_s.at[j], mx_r.at[t], tp=j).wait_send()
        rcopy(qbuf, qrec.at[t], q_s.at[j], q_r.at[t], tp=j).wait_send()
        rcopy(ebuf.at[j], erec.at[t], er_s.at[j], er_r.at[t], tp=j).wait_send()

    @pl.loop(0, E)
    def _(s):
        rcopy(xall.at[t, s], xall.at[t, s], x2_s.at[s], x_r.at[t, s], tp=across).wait_send()
        rcopy(xall.at[t, s], xall.at[t, s], x1_s.at[0, s], x_r.at[t, s], tp=beside).wait_send()
        rcopy(xall.at[across, s], xall.at[across, s], x1_s.at[1, s], x_r.at[across, s], tp=beside).wait_send()

    a_across.wait_send()
    a_beside.wait_send()
    a_fwd.wait_send()


def on_device(
    hidden, mix_gain, proj_x, proj_y, conv_taps, input_gate, decay_gate, decay_param,
    proj_out, conv_state, lru_state, ffn_gain, routes, route_weights,
    expert_gate, expert_up, expert_down, dense_gate, dense_up, dense_down, branch_gate,
):
    E = lax.axis_size("ep")
    T = lax.axis_size("tp")
    M, D = hidden.shape
    C = D // T
    R = proj_x.shape[0]
    N = E * M
    heads, block = input_gate.shape[:2]
    group = max(1, 128 // block)

    experts = expert_gate.shape[0] * E
    capacity = M * routes.shape[1] // experts + 2
    slots = -(-E * capacity // 16) * 16
    G = E // 2
    h = dense_gate.shape[1] // T
    half = -(-2 * h // 128) * 64

    dd = jnp.pad(dense_down.reshape(T, h, C), ((0, 0), (0, half - h), (0, 0)))
    FH = expert_gate.shape[2]
    vm = pl.BlockSpec(memory_space=pltpu.VMEM)
    anyspace = pl.BlockSpec(memory_space=pl.ANY)
    DMA = pltpu.SemaphoreType.DMA
    V = pltpu.VMEM
    rows = min(N, 512)
    scratch = [
        V((E, 1, M), F32), V((1, N), F32), V((heads // group, group * block, 2 * group * block), BF16),
        V((R, C), BF16), V((R, C), BF16), V((C, T * h), BF16), V((C, T * h), BF16),
        V((C, D), BF16), V((D, FH), BF16), V((D, FH), BF16), V((FH, D), BF16), V((T, half, C), BF16),
        V((E, M, R), BF16), V((T, C, 2 * half), BF16), V((T, C, 2 * half), BF16),
        V((E, M, R), BF16), V((G, M, 2 * C), BF16), V((G, M, 2 * C), F32), V((G, M, 2 * C), BF16),
        V((G, M, 2 * C), BF16), V((G, M, 2 * C), BF16), V((E, 1, M), F32), V((M, 2 * C), F32),
        V((T, M, C), BF16), V((T, M, C), BF16), V((M, 128), F32), V((T, M, 128), F32),
        V((T, E, M, C), BF16), V((rows, 2 * half), F32), V((T, N, half), BF16),
        V((slots, D), BF16), V((slots, FH), BF16), V((slots, N), BF16),
        V((T, slots, C), BF16), V((T, slots, C), BF16), V((2, M, C), F32),
        V((G, M, C), BF16), V((G, M, C), F32), V((G, M, C), BF16), V((G, M, C), BF16), V((G, M, C), BF16),
        V((M, C), BF16),
        DMA((10,)),
        DMA((E,)), DMA((E,)), DMA((E,)), DMA((E,)), DMA((G,)), DMA((G,)), DMA((G,)), DMA((G,)),
        DMA((T,)), DMA((T,)), DMA((T,)), DMA((T,)), DMA((T,)), DMA((T,)),
        DMA((G,)), DMA((E,)), DMA((E,)), DMA((2, E)), DMA((T, E)), DMA((3,)), DMA((T,)), DMA((T,)), DMA((T,)),
        DMA((G,)), DMA((G,)), DMA((G,)), DMA((G,)),
    ]
    new_hidden, new_lru, x_new = pl.pallas_call(
        functools.partial(layer_kernel, E, T, slots),
        out_shape=(
            jax.ShapeDtypeStruct((M, C), BF16),
            jax.ShapeDtypeStruct((M, C), F32),
            jax.ShapeDtypeStruct((M, C), BF16),
        ),
        in_specs=[vm] * 12 + [anyspace] * 9,
        out_specs=(vm, vm, vm),
        scratch_shapes=scratch,
        compiler_params=pltpu.CompilerParams(
            collective_id=0, has_side_effects=True, vmem_limit_bytes=60 * 1024 * 1024
        ),
    )(
        hidden, mix_gain[None, :], routes.T, route_weights.T, conv_state.transpose(1, 0, 2), conv_taps,
        input_gate, decay_gate, decay_param[None, :], lru_state,
        ffn_gain[None, :], branch_gate[None, :],
        proj_x, proj_y, dense_gate, dense_up, proj_out, expert_gate[0], expert_up[0], expert_down[0], dd,
    )
    new_conv = jnp.concatenate([conv_state[:, 1:], x_new[:, None, :]], axis=1)
    return (new_hidden, new_lru, new_conv)


def solution(mesh):
    in_specs = (
        P("ep", None),
        P(),
        P("ep", "tp"),
        P("ep", "tp"),
        P(None, "tp"),
        P("tp", None, None),
        P("tp", None, None),
        P("tp"),
        P("tp", None),
        P("ep", None, "tp"),
        P("ep", "tp"),
        P(),
        P("ep", None),
        P("ep", None),
        P("ep", None, "tp"),
        P("ep", None, "tp"),
        P("ep", "tp", None),
        P("tp", "ep"),
        P("tp", "ep"),
        P("ep", "tp"),
        P("tp"),
    )
    out_specs = (P("ep", "tp"), P("ep", "tp"), P("ep", None, "tp"))
    return jax.shard_map(
        on_device, mesh=mesh, in_specs=in_specs, out_specs=out_specs, check_vma=False
    )
```

profile of v0, /device:TPU:0, one launch (start us, length us, event | category | flops | bytes accessed | tf_op | source)
XLA Modules:
  0.0 96.2 jit_solution(15235938616317857006)
XLA Ops:
  0.6 1.3 %broadcast_in_dim.15.mix_gain = bf16[1,2048]{1,0:T(2,128)(2,1)} reshape(bf16[2048]{0:T(1024)(128)(2,1)} %param.22) | data formatting | bytes 8192 | tf_op jit(solution)/shard_map/broadcast_in_dim | solution.py:504
  1.9 1.3 %broadcast_in_dim.17.ffn_gain = bf16[1,2048]{1,0:T(2,128)(2,1)} reshape(bf16[2048]{0:T(1024)(128)(2,1)} %param.32) | data formatting | bytes 8192 | tf_op jit(solution)/shard_map/broadcast_in_dim | solution.py:506
  3.2 0.9 slice.3
  4.1 87.4 %shard_map.220 = (bf16[64,512]{1,0:T(8,128)(2,1)}, f32[64,512]{1,0:T(8,128)}, bf16[64,512]{1,0:T(8,128)(2,1)}) custom-call(bf16[64,2048]{1,0:T(8,128)(2,1)} %hidden.1, bf16[1,2048]{1,0:T(2,128)(2,1)} %broadcast_in_dim.15.mix_gain, s32[2,64]{1,0:T(2,128)} %bitcast.18, f32[2,64]{1,0:T(2,128)} %bitcast.19, bf16[3,64,512]{2,1,0:T(8,128)(2,1)} %bitcast.14, ...), custom_call_target="tpu_custom_call" | custom-call | tf_op jit(solution)/shard_map/pallas_call | solution.py:490
  91.6 1.5 %pad_maximum_fusion = bf16[64,3,512]{2,0,1:T(8,128)(2,1)} fusion(bf16[64,1,512]{2,0,1:T(8,128)(2,1)} %bitcast.15, bf16[64,2,512]{2,0,1:T(8,128)(2,1)S(1)} %slice.3), kind=kLoop, calls=%fused_computation | loop fusion | flops 98304 | bytes 393216 | tf_op jit(solution)/shard_map/concatenate | solution.py:509
  93.1 1.5 %copy.26 = bf16[64,512]{1,0:T(8,128)(2,1)} copy(bf16[64,512]{1,0:T(8,128)(2,1)} %get-tuple-element.12) | data formatting | bytes 131072
  94.6 1.6 %copy.27 = f32[64,512]{1,0:T(8,128)} copy(f32[64,512]{1,0:T(8,128)} %get-tuple-element.13) | data formatting | bytes 262144
where the time goes:
time: 96.5 us; the launch traced here: 96.2 us
  Pallas kernels  87.4 us (91%)
  local copies, waits for them, and re-layouts  6.53 us (7%)
  other arithmetic  1.54 us (2%)
    pallas_call x1, Pallas kernels, on_device(): pl.pallas_call(functools.partial(layer_kernel, E, T, slots), out_shape=(j...  87.4 us
    unnamed x2, local copies, waits for them, and re-layouts  3.04 us

commit v1 on v0

v1 whole, which is shorter than its diff:
```python
import functools

import jax
import jax.numpy as jnp
from jax import lax
from jax.experimental import pallas as pl
from jax.experimental.pallas import tpu as pltpu
from jax.sharding import PartitionSpec as P

epsilon = 1e-06
decay_scale = 8.0
MESH = pl.DeviceIdType.MESH
F32 = jnp.float32
BF16 = jnp.bfloat16


def dot(a, b):
    return jnp.dot(a, b, preferred_element_type=F32)


def layer_kernel(
    E, T, cap,
    hidden, mix_gain, routes, weights, conv_old, taps, ig, dgate, decay_param, lru, ffn_gain, branch,
    wx_h, wy_h, dg_h, du_h, po_h, eg_h, eu_h, ed_h, dd_h,
    new_hidden, new_lru, conv_new,
    ct, w_ref, bd, wx, wy, dg, du, po, eg, eu, ed, dd, nb, dwp, dwr, spread, pm, pacc, yrec, zout, zrec, ctr, acc,
    mbuf, mrec, srow, prow, xall, aall, xe, hid, sel, own_sel, w_slot, s_slot,
    ebuf, erec, epart, ex, exr, eo, eor, dtmp, om, dacc, orm, oz, ozr, summed_ref,
    load_sem, nb_s, nb_r, ct_s, ct_r, pm_s, pm_r, pz_s, pz_r, dw_s, dw_r, mx_s, mx_r, q_s, q_r,
    xr_s, xf_s, xs_s, xd_s, x_r, a_s, a_r, ed_s, ed_r, ex_s, ex_r, eo_s, eo_r, om_s, om_r, oz_s, oz_r,
):
    e = lax.axis_index("ep")
    t = lax.axis_index("tp")
    M, D = hidden.shape
    C = D // T
    R = wx.shape[0]
    G = E // 2
    g0 = e // 2
    par = lax.rem(e, 2)
    mate = e + 1 - 2 * par
    own_cols = pl.ds(pl.multiple_of(t * C, 128), C)

    def ep_peer(k):
        return lax.rem(e + k, E)

    def ep_from(k):
        return lax.rem(e + E - k, E)

    def group(k):
        return lax.rem(g0 + k, G)

    def rail_from(k):
        return 2 * lax.rem(g0 + G - k, G) + par

    def mate_of(s):
        return s + 1 - 2 * lax.rem(s, 2)

    def peer_group(k):
        if G & (G - 1):
            return lax.rem(g0 + k, G)
        g, bit = 0, 1
        while bit < G:
            g = g + bit * lax.rem(g0 // bit + k // bit, 2)
            bit *= 2
        return g

    def tp_peer(k):
        return lax.rem(t + k, T)

    across = lax.rem(t + T // 2, T)
    beside = t + 1 - 2 * lax.rem(t, 2)
    diagonal = lax.rem(beside + T // 2, T)

    loads = [
        pltpu.make_async_copy(src, dst, load_sem.at[i])
        for i, (src, dst) in enumerate(
            ((po_h, po), (eg_h, eg), (eu_h, eu), (ed_h, ed), (dd_h, dd),
             (wx_h, wx), (wy_h, wy), (dg_h, dg), (du_h, du))
        )
    ]
    own_dw = pltpu.make_async_copy(dwp.at[t], dwr.at[t], load_sem.at[9])
    for i in (5, 6, 7, 8, 0):
        loads[i].start()

    def rcopy(src, dst, s, r, ep=None, tp=None):
        return pltpu.make_async_remote_copy(
            src_ref=src, dst_ref=dst, send_sem=s, recv_sem=r,
            device_id=(e if ep is None else ep, t if tp is None else tp),
            device_id_type=MESH,
        )

    barrier = pltpu.get_barrier_semaphore()

    @pl.loop(1, E)
    def _(k):
        pl.semaphore_signal(barrier, inc=1, device_id=(ep_peer(k), t), device_id_type=MESH)

    for k in range(1, T):
        pl.semaphore_signal(barrier, inc=1, device_id=(e, tp_peer(k)), device_id_type=MESH)
    hf = hidden[...].astype(F32)
    inv = lax.rsqrt(jnp.mean(hf * hf, axis=-1, keepdims=True) + epsilon)
    normed = (hf * inv * mix_gain[...].reshape(1, D).astype(F32)).astype(BF16)
    for p in range(E):
        nb[p] = normed[:, p * R:(p + 1) * R]
    for p in range(E):
        ct[p] = jnp.sum(jnp.where(routes[...] == p, weights[...], 0.0), axis=0, keepdims=True)
    pl.semaphore_wait(barrier, E - 1 + T - 1)

    @pl.loop(1, E)
    def _(k):
        p = ep_peer(k)
        rcopy(nb.at[p], spread.at[e], nb_s.at[p], nb_r.at[e], ep=p).start()
        rcopy(ct.at[p], ctr.at[e], ct_s.at[p], ct_r.at[e], ep=p).start()

    loads[7].wait()
    loads[8].wait()
    h = dg.shape[1] // T
    half = dwp.shape[2] // 2
    if half != h:
        dwp[...] = jnp.zeros_like(dwp)
    for j in range(T):
        dwp[j, :, :h] = dg[:, j * h:(j + 1) * h]
        dwp[j, :, half:half + h] = du[:, j * h:(j + 1) * h]
    own_dw.start()
    for k in range(1, T):
        j = tp_peer(k)
        rcopy(dwp.at[j], dwr.at[t], dw_s.at[j], dw_r.at[t], tp=j).start()
    for l in loads[1:5]:
        l.start()

    spread[e] = nb[e]
    loads[5].wait()
    loads[6].wait()

    def arrive(s):
        rcopy(nb.at[s], spread.at[s], nb_s.at[s], nb_r.at[s], ep=s).wait_recv()

    def share(g):
        blk = spread[2 * g + 1 - par]
        pm[g, :, :C] = dot(blk, wx[...]).astype(BF16)
        pm[g, :, C:] = dot(blk, wy[...]).astype(BF16)
        rcopy(pm.at[g], yrec.at[g], pm_s.at[g], pm_r.at[g], ep=mate).start()
        blk = spread[2 * g + par]
        pacc[g, :, :C] = dot(blk, wx[...])
        pacc[g, :, C:] = dot(blk, wy[...])

    def pass_on(g):
        rcopy(pm.at[g], yrec.at[g], pm_s.at[g], pm_r.at[g], ep=mate).wait_recv()
        zout[g] = (pacc[g] + yrec[g].astype(F32)).astype(BF16)
        rcopy(zout.at[g], zrec.at[g0], pz_s.at[g], pz_r.at[g0], ep=2 * g + par).start()

    @pl.loop(1, G)
    def _(k):
        g = group(k)
        arrive(2 * g + 1 - par)
        arrive(2 * g + par)
        share(g)

        @pl.when(k > 1)
        def _():
            pass_on(group(k - 1))

    arrive(mate)
    share(g0)
    pass_on(group(G - 1))

    @pl.loop(1, E)
    def _(k):
        s = ep_from(k)
        rcopy(ct.at[s], ctr.at[s], ct_s.at[s], ct_r.at[s], ep=s).wait_recv()

    ctr[e] = ct[e]
    for s in range(E):
        w_ref[s // 2, :, s % 2 * M:(s % 2 + 1) * M] = ctr[s]
    bd[...] = jnp.zeros_like(bd)
    block = ig.shape[1]
    width = bd.shape[1]
    per = width // block
    for i in range(ig.shape[0]):
        lo = i % per * block
        bd[i // per, lo:lo + block, lo:lo + block] = ig[i]
        bd[i // per, lo:lo + block, width + lo:width + lo + block] = dgate[i]
    def before(n):
        row = lax.broadcasted_iota(jnp.int32, (n, n), 0)
        col = lax.broadcasted_iota(jnp.int32, (n, n), 1)
        return ((row < col) & (row // M == col // M)).astype(F32).astype(BF16)

    def rank_of(m, earlier):
        rows = max(16, m.shape[0])
        return dot(jnp.broadcast_to(m, (rows, m.shape[1])).astype(BF16), earlier)[0:1]

    pair = 2 * M
    lower = before(pair)
    slot = lax.broadcasted_iota(jnp.int32, (2 * cap, pair), 0)
    first_slot = lax.broadcasted_iota(jnp.int32, (2 * cap, pair), 1) // M * cap
    slot = (slot - first_slot).astype(F32)

    @pl.loop(0, G)
    def _(g):
        w_row = w_ref[g]
        m = (w_row > 0.0).astype(F32)
        hit = (slot == rank_of(m, lower)).astype(F32) * m
        sel[g] = hit.astype(BF16)
        w_slot[g] = jnp.broadcast_to(jnp.sum(hit * w_row, axis=1, keepdims=True), w_slot.shape[1:])

    lower = before(M)
    slot = lax.broadcasted_iota(jnp.int32, (cap, M), 0).astype(F32)

    def own_hit(p):
        m = (ct[p] > 0.0).astype(F32)
        return (slot == rank_of(m, lower)).astype(F32) * m

    @pl.loop(0, G)
    def _(g):
        own_sel[g] = jnp.concatenate([own_hit(2 * g), own_hit(2 * g + 1)], axis=0).astype(BF16)

    rcopy(pm.at[g0], yrec.at[g0], pm_s.at[g0], pm_r.at[g0], ep=mate).wait_recv()
    acc[...] = pacc[g0] + yrec[g0].astype(F32)

    @pl.loop(1, G)
    def _(k):
        g = group(k)
        rcopy(zout.at[g], zrec.at[g], pz_s.at[g], pz_r.at[g], ep=2 * g + par).wait_recv()
        acc[...] += zrec[g].astype(F32)

    x_b = acc[:, :C].astype(BF16)
    y_b = acc[:, C:].astype(BF16)
    for i in range(1, conv_old.shape[0]):
        conv_new[i - 1] = conv_old[i]
    conv_new[conv_old.shape[0] - 1] = x_b
    conv_pre = conv_old[0].astype(F32) * taps[0:1, :].astype(F32)
    for i in range(1, taps.shape[0] - 1):
        conv_pre = conv_pre + conv_old[i].astype(F32) * taps[i:i + 1, :].astype(F32)
    conv = (conv_pre + x_b.astype(F32) * taps[taps.shape[0] - 1:, :].astype(F32)).astype(BF16)
    gi, gd = [], []
    for i in range(C // width):
        g = dot(conv[:, i * width:(i + 1) * width], bd[i])
        gi.append(g[:, :width])
        gd.append(g[:, width:])
    gate_in = jax.nn.sigmoid(jnp.concatenate(gi, axis=1))
    gate_dec = jax.nn.sigmoid(jnp.concatenate(gd, axis=1))
    dp = decay_param[...]
    log_decay = decay_scale * gate_dec * (jnp.minimum(dp, 0.0) - jnp.log1p(jnp.exp(-jnp.abs(dp))))
    decay = jnp.exp(log_decay)
    inject = jnp.sqrt(-jnp.tanh(log_decay) * (1.0 + decay * decay))
    state = decay * lru[...] + inject * gate_in * conv.astype(F32)
    new_lru[...] = state
    gated = (state * jax.nn.gelu(y_b.astype(F32), approximate=True)).astype(BF16)

    loads[0].wait()
    order = [tp_peer(k) for k in (2, 3, 1)] if T == 4 else [tp_peer(k) for k in range(1, T)]
    for j in order:
        cols = pl.ds(pl.multiple_of(j * C, 128), C)
        mbuf[j] = dot(gated, po[:, cols]).astype(BF16)
        rcopy(mbuf.at[j], mrec.at[t], mx_s.at[j], mx_r.at[t], tp=j).start()
    mixer = dot(gated, po[:, own_cols]).astype(BF16).astype(F32)
    for j in reversed(order):
        rcopy(mbuf.at[j], mrec.at[j], mx_s.at[j], mx_r.at[j], tp=j).wait_recv()
        mixer = mixer + mrec[j].astype(F32)
    summed = (hidden[:, own_cols].astype(F32) + mixer).astype(BF16)
    summed_ref[...] = summed
    sf = summed.astype(F32)
    ssq = jnp.sum(sf * sf, axis=1, keepdims=True)
    same = lax.broadcasted_iota(jnp.int32, (M, M), 0) == lax.broadcasted_iota(jnp.int32, (M, M), 1)
    srow[t, e] = jnp.sum(jnp.where(same, ssq, 0.0), axis=0, keepdims=True)

    def each_other(fn):
        @pl.loop(1, E * T)
        def _(k):
            r = lax.rem(e * T + t + k, E * T)
            fn(r // T, lax.rem(r, T))

    def scale_to(p, q):
        return rcopy(srow.at[t, e], srow.at[t, e], q_s.at[q, p], q_r.at[t, e], ep=p, tp=q)

    each_other(lambda p, q: scale_to(p, q).start())
    xall[t, e] = (sf * ffn_gain[own_cols].reshape(1, C).astype(F32)).astype(BF16)

    core = lax.rem(t, 2)
    to_across = core * (across - t)
    to_mate = (1 - core) * (mate - e)
    first = dict(ep=e + to_mate, tp=t + to_across)
    second = dict(ep=e + core * (mate - e), tp=t + (1 - core) * (across - t))

    def slice_a(k):
        return t, 2 * peer_group(k) + par

    def slice_b(k):
        q, s = slice_a(k)
        return q + to_across, s + (1 - core) * (mate_of(s) - s)

    def slice_c(k):
        q, s = slice_a(k)
        return q + (1 - core) * (across - t), s + core * (mate_of(s) - s)

    def slice_d(k):
        q, s = slice_a(k)
        return across, mate_of(s)

    def move(at, sem, **to):
        q, s = at
        return rcopy(xall.at[q, s], xall.at[q, s], sem, x_r.at[q, s], **to)

    def landed(at):
        move(at, xr_s.at[0], ep=mate).wait_recv()

    def rail(k):
        return move(slice_a(0), xr_s.at[k], ep=2 * peer_group(k) + par)

    def first_a(k):
        return move(slice_a(k), xf_s.at[k], **first)

    def second_a(k):
        return move(slice_a(k), xs_s.at[0, k], **second)

    def second_b(k):
        return move(slice_b(k), xs_s.at[1, k], **second)

    def beside_of(i, k):
        return move((slice_a, slice_b, slice_c, slice_d)[i](k), xd_s.at[i, k], tp=beside)

    def pass_a(k):
        first_a(k).start()
        second_a(k).start()
        beside_of(0, k).start()

    @pl.loop(1, G)
    def _(k):
        rail(k).start()

    pass_a(0)
    own_dw.wait()
    for j in order:
        rcopy(dwp.at[j], dwr.at[j], dw_s.at[j], dw_r.at[j], tp=j).wait_recv()
    square = (
        lax.broadcasted_iota(jnp.int32, (pair, pair), 0) == lax.broadcasted_iota(jnp.int32, (pair, pair), 1)
    )

    def a_copy(q, g, i, to):
        return rcopy(aall.at[q, g], aall.at[q, g], a_s.at[i, g], a_r.at[q, g], tp=to)

    def pair_in(k):
        g = peer_group(k)
        for i in range(2):
            s = 2 * g + i
            total = jnp.zeros((1, M), F32)
            for q in range(T):
                @pl.when((s != e) | (q != t))
                def _():
                    rcopy(srow.at[q, s], srow.at[q, s], q_s.at[q, s], q_r.at[q, s], ep=mate).wait_recv()

                total = total + srow[q, s]
            prow[:, i * M:(i + 1) * M] = total
            landed((beside, s))
            landed((diagonal, s))
        scale_row = lax.rsqrt(prow[...] * (1.0 / D) + epsilon)
        scale = jnp.sum(jnp.where(square, scale_row, 0.0), axis=1, keepdims=True)
        h = None
        for q in range(T):
            part = dot(xall[q, pl.ds(2 * g, 2)].reshape(pair, C), dwr[q])
            h = part if h is None else h + part
        h = h * scale
        half = h.shape[1] // 2
        act = jax.nn.silu(h) * pltpu.roll(h, half, axis=1)
        aall[t, g] = act[:, :half].astype(BF16)
        a_copy(t, g, 0, across).start()
        a_copy(t, g, 1, beside).start()
        pick = sel[g]
        for q in range(T):
            xe[g, :, q * C:(q + 1) * C] = dot(pick, xall[q, pl.ds(2 * g, 2)].reshape(pair, C)).astype(BF16)
        s_slot[g] = jnp.broadcast_to(
            jnp.sum(pick.astype(F32) * scale_row, axis=1, keepdims=True), s_slot.shape[1:]
        )

    def a_forward(k):
        g = peer_group(k)
        a_copy(across, g, 0, across).wait_recv()
        a_copy(across, g, 2, beside).start()

    gate = jax.nn.sigmoid(branch[...])

    def dense(k):
        g = peer_group(k)
        a_copy(beside, g, 1, beside).wait_recv()
        a_copy(diagonal, g, 2, beside).wait_recv()
        d = dot(aall[0, g], dd[0])
        for q in range(1, T):
            d = d + dot(aall[q, g], dd[q])
        dtmp[...] = (d * gate).reshape(2, M, C)
        om[g] = dtmp[1 - par].astype(BF16)
        rcopy(om.at[g], orm.at[g], om_s.at[g], om_r.at[g], ep=mate).start()
        dacc[g] = dtmp[par]

    def dense_on(k):
        g = peer_group(k)
        rcopy(om.at[g], orm.at[g], om_s.at[g], om_r.at[g], ep=mate).wait_recv()
        oz[g] = (dacc[g] + orm[g].astype(F32)).astype(BF16)
        rcopy(oz.at[g], ozr.at[g0], oz_s.at[g], oz_r.at[g0], ep=2 * g + par).start()

    for l in loads[4:5]:
        l.wait()

    @pl.loop(0, G + 2)
    def _(k):
        @pl.when((k >= 1) & (k < G))
        def _():
            landed(slice_a(k))
            pass_a(k)

        @pl.when((k >= 1) & (k <= G))
        def _():
            landed(slice_b(k - 1))
            second_b(k - 1).start()
            beside_of(1, k - 1).start()
            landed(slice_c(k - 1))
            beside_of(2, k - 1).start()

        @pl.when(k >= 2)
        def _():
            landed(slice_d(k - 2))
            beside_of(3, k - 2).start()
            pair_in(k - 2)

        @pl.when(k >= 3)
        def _():
            a_forward(k - 3)

        @pl.when(k >= 4)
        def _():
            dense(k - 4)

    loads[1].wait()
    loads[2].wait()
    FH = eg.shape[1]
    nch = 256 if FH % 256 == 0 else FH
    slots = E * cap

    @pl.loop(0, FH // nch)
    def _(n):
        cols = pl.ds(pl.multiple_of(n * nch, 128), nch)
        rows_in = xe[...].reshape(slots, D)
        scale = s_slot[...].reshape(slots, 128)[:, 0:1]
        g = dot(rows_in, eg[:, cols]) * scale
        u = dot(rows_in, eu[:, cols]) * scale
        hid[:, cols] = (jax.nn.silu(g) * u).astype(BF16)

    loads[3].wait()

    def down(j):
        return dot(hid[...], ed[:, pl.ds(pl.multiple_of(j * C, 128), C)])

    def e_copy(i):
        return rcopy(ebuf.at[i], erec.at[i], ed_s.at[i], ed_r.at[i], tp=beside)

    for i, j in ((1, diagonal), (0, beside)):
        ebuf[i] = down(j).reshape(G, 2 * cap, C).astype(BF16)
        e_copy(i).start()
    epart[1] = down(across).reshape(G, 2 * cap, C)
    epart[0] = down(t).reshape(G, 2 * cap, C)
    a_forward(G - 1)

    def ex_copy(g):
        return rcopy(ex.at[g], exr.at[g], ex_s.at[g], ex_r.at[g], tp=across)

    e_copy(1).wait_recv()

    @pl.loop(0, G)
    def _(k):
        g = peer_group(G - 1 - k)
        ex[g] = (epart[1, g] + erec[1, g].astype(F32)).astype(BF16)
        ex_copy(g).start()

    for k in range(max(0, G - 2), G):
        dense(k)
    e_copy(0).wait_recv()

    @pl.loop(1, G)
    def _(k):
        dense_on(k)


    def eo_copy(s, p):
        return rcopy(eo.at[s], eor.at[p], eo_s.at[s], eo_r.at[p], ep=s)

    @pl.loop(0, G)
    def _(k):
        g = peer_group(G - 1 - k)
        ex_copy(g).wait_recv()
        red = epart[0, g] + erec[0, g].astype(F32) + exr[g].astype(F32)
        red = red.astype(BF16).astype(F32) * w_slot[g][:, 0:1]
        eo[pl.ds(2 * g, 2)] = red.reshape(2, cap, C).astype(BF16)
        for i in range(2):
            s = 2 * g + i

            @pl.when(s != e)
            def _():
                eo_copy(s, e).start()

    eor[e] = eo[e]
    rcopy(om.at[g0], orm.at[g0], om_s.at[g0], om_r.at[g0], ep=mate).wait_recv()
    acc[:, :C] = summed_ref[...].astype(F32) + dacc[g0] + orm[g0].astype(F32)

    @pl.loop(1, G)
    def _(k):
        g = peer_group(k)
        rcopy(oz.at[g], ozr.at[g], oz_s.at[g], oz_r.at[g], ep=2 * g + par).wait_recv()
        acc[:, :C] += ozr[g].astype(F32)


    @pl.loop(1, E)
    def _(k):
        p = ep_from(k)
        eo_copy(p, p).wait_recv()

    picked = eor[...].astype(F32).reshape(slots, C).astype(BF16)
    new_hidden[...] = (
        acc[:, :C] + lax.dot_general(
            own_sel[...].reshape(slots, M), picked, (((0,), (0,)), ((), ())), preferred_element_type=F32
        )
    ).astype(BF16)

    @pl.loop(1, E)
    def _(k):
        p = ep_peer(k)
        rcopy(nb.at[p], spread.at[e], nb_s.at[p], nb_r.at[e], ep=p).wait_send()
        rcopy(ct.at[p], ctr.at[e], ct_s.at[p], ct_r.at[e], ep=p).wait_send()

    @pl.loop(0, G)
    def _(k):
        g = peer_group(k)
        rcopy(pm.at[g], yrec.at[g], pm_s.at[g], pm_r.at[g], ep=mate).wait_send()
        rcopy(om.at[g], orm.at[g], om_s.at[g], om_r.at[g], ep=mate).wait_send()
        first_a(k).wait_send()
        second_a(k).wait_send()
        second_b(k).wait_send()
        for i in range(4):
            beside_of(i, k).wait_send()
        a_copy(t, g, 0, across).wait_send()
        a_copy(t, g, 1, beside).wait_send()
        a_copy(across, g, 2, beside).wait_send()
        ex_copy(g).wait_send()

    @pl.loop(1, G)
    def _(k):
        g = group(k)
        p = 2 * g + par
        rcopy(zout.at[g], zrec.at[g0], pz_s.at[g], pz_r.at[g0], ep=p).wait_send()
        rcopy(oz.at[g], ozr.at[g0], oz_s.at[g], oz_r.at[g0], ep=p).wait_send()
        rail(k).wait_send()

    @pl.loop(1, E)
    def _(k):
        eo_copy(ep_peer(k), e).wait_send()

    each_other(lambda p, q: scale_to(p, q).wait_send())
    for j in order:
        rcopy(dwp.at[j], dwr.at[t], dw_s.at[j], dw_r.at[t], tp=j).wait_send()
        rcopy(mbuf.at[j], mrec.at[t], mx_s.at[j], mx_r.at[t], tp=j).wait_send()
    for i in range(2):
        e_copy(i).wait_send()


def store_kernel(a, b, c, a_out, b_out, c_out, sems):
    copies = [
        pltpu.make_async_copy(src, dst, sems.at[i])
        for i, (src, dst) in enumerate(((a, a_out), (b, b_out), (c, c_out)))
    ]
    for copy in copies:
        copy.start()
    for copy in copies:
        copy.wait()


def on_device(
    hidden, mix_gain, proj_x, proj_y, conv_taps, input_gate, decay_gate, decay_param,
    proj_out, conv_state, lru_state, ffn_gain, routes, route_weights,
    expert_gate, expert_up, expert_down, dense_gate, dense_up, dense_down, branch_gate,
):
    E = lax.axis_size("ep")
    T = lax.axis_size("tp")
    M, D = hidden.shape
    C = D // T
    R = proj_x.shape[0]
    N = E * M
    heads, block = input_gate.shape[:2]
    group = max(1, 128 // block)

    experts = expert_gate.shape[0] * E
    cap = -(-(M * routes.shape[1] // experts + 2) // 8) * 8
    slots = E * cap
    G = E // 2
    h = dense_gate.shape[1] // T
    half = -(-2 * h // 128) * 64

    dd = jnp.pad(dense_down.reshape(T, h, C), ((0, 0), (0, half - h), (0, 0)))
    FH = expert_gate.shape[2]
    vm = pl.BlockSpec(memory_space=pltpu.VMEM)
    anyspace = pl.BlockSpec(memory_space=pl.ANY)
    DMA = pltpu.SemaphoreType.DMA
    V = pltpu.VMEM
    scratch = [
        V((E, 1, M), F32), V((G, 1, 2 * M), F32), V((heads // group, group * block, 2 * group * block), BF16),
        V((R, C), BF16), V((R, C), BF16), V((C, T * h), BF16), V((C, T * h), BF16),
        V((C, D), BF16), V((D, FH), BF16), V((D, FH), BF16), V((FH, D), BF16), V((T, half, C), BF16),
        V((E, M, R), BF16), V((T, C, 2 * half), BF16), V((T, C, 2 * half), BF16),
        V((E, M, R), BF16), V((G, M, 2 * C), BF16), V((G, M, 2 * C), F32), V((G, M, 2 * C), BF16),
        V((G, M, 2 * C), BF16), V((G, M, 2 * C), BF16), V((E, 1, M), F32), V((M, 2 * C), F32),
        V((T, M, C), BF16), V((T, M, C), BF16), V((T, E, 1, M), F32), V((1, 2 * M), F32),
        V((T, E, M, C), BF16), V((T, G, 2 * M, half), BF16),
        V((G, 2 * cap, D), BF16), V((slots, FH), BF16), V((G, 2 * cap, 2 * M), BF16),
        V((G, 2 * cap, M), BF16), V((G, 2 * cap, 128), F32), V((G, 2 * cap, 128), F32),
        V((2, G, 2 * cap, C), BF16), V((2, G, 2 * cap, C), BF16), V((2, G, 2 * cap, C), F32),
        V((G, 2 * cap, C), BF16), V((G, 2 * cap, C), BF16), V((E, cap, C), BF16), V((E, cap, C), BF16),
        V((2, M, C), F32),
        V((G, M, C), BF16), V((G, M, C), F32), V((G, M, C), BF16), V((G, M, C), BF16), V((G, M, C), BF16),
        V((M, C), BF16),
        DMA((10,)),
        DMA((E,)), DMA((E,)), DMA((E,)), DMA((E,)), DMA((G,)), DMA((G,)), DMA((G,)), DMA((G,)),
        DMA((T,)), DMA((T,)), DMA((T,)), DMA((T,)), DMA((T, E)), DMA((T, E)),
        DMA((G,)), DMA((G,)), DMA((2, G)), DMA((4, G)), DMA((T, E)), DMA((3, G)), DMA((T, G)),
        DMA((2,)), DMA((2,)), DMA((G,)), DMA((G,)), DMA((E,)), DMA((E,)),
        DMA((G,)), DMA((G,)), DMA((G,)), DMA((G,)),
    ]
    outs = pl.pallas_call(
        functools.partial(layer_kernel, E, T, cap),
        out_shape=(
            jax.ShapeDtypeStruct((M, C), BF16),
            jax.ShapeDtypeStruct((M, C), F32),
            jax.ShapeDtypeStruct((conv_state.shape[1], M, C), BF16),
        ),
        in_specs=[vm] * 12 + [anyspace] * 9,
        out_specs=(vm, vm, vm),
        scratch_shapes=scratch,
        compiler_params=pltpu.CompilerParams(
            collective_id=0, has_side_effects=True, vmem_limit_bytes=60 * 1024 * 1024
        ),
    )(
        hidden, mix_gain, routes.T, route_weights.T, conv_state.transpose(1, 0, 2), conv_taps,
        input_gate, decay_gate, decay_param[None, :], lru_state,
        ffn_gain, branch_gate[None, :],
        proj_x, proj_y, dense_gate, dense_up, proj_out, expert_gate[0], expert_up[0], expert_down[0], dd,
    )
    new_hidden, new_lru, new_conv = pl.pallas_call(
        store_kernel,
        out_shape=tuple(jax.ShapeDtypeStruct(o.shape, o.dtype) for o in outs),
        in_specs=[vm] * 3,
        out_specs=(anyspace,) * 3,
        scratch_shapes=[DMA((3,))],
    )(*outs)
    return (new_hidden, new_lru, new_conv.transpose(1, 0, 2))


def solution(mesh):
    in_specs = (
        P("ep", None),
        P(),
        P("ep", "tp"),
        P("ep", "tp"),
        P(None, "tp"),
        P("tp", None, None),
        P("tp", None, None),
        P("tp"),
        P("tp", None),
        P("ep", None, "tp"),
        P("ep", "tp"),
        P(),
        P("ep", None),
        P("ep", None),
        P("ep", None, "tp"),
        P("ep", None, "tp"),
        P("ep", "tp", None),
        P("tp", "ep"),
        P("tp", "ep"),
        P("ep", "tp"),
        P("tp"),
    )
    out_specs = (P("ep", "tp"), P("ep", "tp"), P("ep", None, "tp"))
    return jax.shard_map(
        on_device, mesh=mesh, in_specs=in_specs, out_specs=out_specs, check_vma=False
    )
```

time: 96.5 us -> 82.8 us (0.86)
  local copies, waits for them, and re-layouts: 6.53 us -> 0 us
  Pallas kernels: 87.4 us -> 82 us
  other arithmetic: 1.54 us -> 0 us
    pallas_call x1 -> x2, Pallas kernels: 87.4 us -> 82 us  [the longest x1 80.2 us: on_device(): pl.pallas_call(functools.partial(layer_kernel, E, T, cap), out_shape=(jax...]
    unnamed x2 -> x0, local copies, waits for them, and re-layouts: 3.04 us -> none
    broadcast_in_dim x2 -> x0, local copies, waits for them, and re-layouts: 2.58 us -> none  [the longest x1 1.29 us: on_device(): mix_gain[None, :]]
    concatenate x1 -> x0, other arithmetic: 1.54 us -> none  [on_device(): new_conv = jnp.concatenate([conv_state[:, 1:], x_new[:, None, :]], axis=1)]
where the time goes in v1:
time: 82.8 us; the launch traced here: 82.7 us
  Pallas kernels  82 us (99%)
    pallas_call x1, Pallas kernels, on_device(): pl.pallas_call(functools.partial(layer_kernel, E, T, cap), out_shape=(jax...  80.2 us
    pallas_call x1, Pallas kernels, on_device(): pl.pallas_call(store_kernel, out_shape=tuple((jax.ShapeDtypeStruct(o.shap...  1.79 us

profile of v1, /device:TPU:0, one launch (start us, length us, event | category | flops | bytes accessed | tf_op | source)
XLA Modules:
  0.0 82.7 jit_solution(18112628116490321751)
XLA Ops:
  0.6 80.2 %shard_map.220 = (bf16[64,512]{1,0:T(8,128)(2,1)}, f32[64,512]{1,0:T(8,128)}, bf16[3,64,512]{2,1,0:T(8,128)(2,1)}) custom-call(bf16[64,2048]{1,0:T(8,128)(2,1)} %hidden.1, bf16[2048]{0:T(1024)(128)(2,1)} %mix_gain.1, s32[2,64]{1,0:T(2,128)} %bitcast.17, f32[2,64]{1,0:T(2,128)} %bitcast.18, bf16[3,64,512]{2,1,0:T(8,128)(2,1)} %bitcast.14, ...), custom_call_target="tpu_custom_call" | custom-call | tf_op jit(solution)/shard_map/pallas_call | solution.py:624
  80.9 1.8 %shard_map.221 = (bf16[64,512]{1,0:T(8,128)(2,1)}, f32[64,512]{1,0:T(8,128)}, bf16[3,64,512]{2,1,0:T(8,128)(2,1)}) custom-call(bf16[64,512]{1,0:T(8,128)(2,1)} %get-tuple-element.9.a, f32[64,512]{1,0:T(8,128)} %get-tuple-element.10.b, bf16[3,64,512]{2,1,0:T(8,128)(2,1)} %get-tuple-element.11.c), custom_call_target="tpu_custom_call" | custom-call | tf_op jit(solution)/shard_map/pallas_call | solution.py:643

commit v2 on v1

v2 whole, which is shorter than its diff:
```python
import functools

import jax
import jax.numpy as jnp
from jax import lax
from jax.experimental import pallas as pl
from jax.experimental.pallas import tpu as pltpu
from jax.sharding import PartitionSpec as P

epsilon = 1e-06
decay_scale = 8.0
MESH = pl.DeviceIdType.MESH
F32 = jnp.float32
BF16 = jnp.bfloat16


def dot(a, b):
    return jnp.dot(a, b, preferred_element_type=F32)


def layer_kernel(
    E, T, cap,
    hidden, mix_gain, routes, weights, conv_old, taps, ig, dgate, decay_param, lru, ffn_gain, branch,
    wx_h, wy_h, dg_h, du_h, po_h, eg_h, eu_h, ed_h, dd_h,
    new_hidden, new_lru, conv_new,
    ct, w_ref, bd, wall, dg, du, po, eg, eu, ed, dd, nb, dwp, dwr, xin, zf, zout, zrec, ctr, acc,
    mbuf, mrec, srow, prow, xall, aall, xe, hid, sel, own_sel, w_slot, s_slot,
    ebuf, erec, epart, ex, exr, eo, eor, dtmp, om, dacc, orm, oz, ozr, summed_ref,
    load_sem, w_l, w_s, w_r, nb_s, nb_r, nf_s, nf_r, ct_s, ct_r, pz_s, pz_r, dw_s, dw_r, mx_s, mx_r, q_s, q_r,
    x_s, x_r, xb_r, a_s, a_r, ab_r, ed_s, ed_r, ex_s, ex_r, eo_s, eo_r, om_s, om_r, oz_s, oz_r,
):
    e = lax.axis_index("ep")
    t = lax.axis_index("tp")
    M, D = hidden.shape
    C = D // T
    R = wx_h.shape[0]
    chunks, CW = wall.shape[0], wall.shape[3]
    G = E // 2
    g0 = e // 2
    par = lax.rem(e, 2)
    mate = e + 1 - 2 * par
    own_cols = pl.ds(pl.multiple_of(t * C, 128), C)

    def ep_peer(k):
        return lax.rem(e + k, E)

    def ep_from(k):
        return lax.rem(e + E - k, E)

    def group(k):
        return lax.rem(g0 + k, G)

    def rail_from(k):
        return 2 * lax.rem(g0 + G - k, G) + par

    def mate_of(s):
        return s + 1 - 2 * lax.rem(s, 2)

    def peer_group(k):
        if G & (G - 1):
            return lax.rem(g0 + k, G)
        g, bit = 0, 1
        while bit < G:
            g = g + bit * lax.rem(g0 // bit + k // bit, 2)
            bit *= 2
        return g

    def tp_peer(k):
        return lax.rem(t + k, T)

    across = lax.rem(t + T // 2, T)
    beside = t + 1 - 2 * lax.rem(t, 2)
    diagonal = lax.rem(beside + T // 2, T)

    loads = [
        pltpu.make_async_copy(src, dst, load_sem.at[i])
        for i, (src, dst) in enumerate(
            ((po_h, po), (eg_h, eg), (eu_h, eu), (ed_h, ed), (dd_h, dd),
             (dg_h, dg), (du_h, du))
        )
    ]
    own_dw = pltpu.make_async_copy(dwp.at[t], dwr.at[t], load_sem.at[7])

    def w_load(i):
        src, col = (wx_h, i * CW) if i * CW < C else (wy_h, i * CW - C)
        return pltpu.make_async_copy(src.at[:, pl.ds(col, CW)], wall.at[i, par], w_l.at[0])

    for i in range(chunks):
        w_load(i).start()
    for i in (5, 6, 0):
        loads[i].start()

    def rcopy(src, dst, s, r, ep=None, tp=None):
        return pltpu.make_async_remote_copy(
            src_ref=src, dst_ref=dst, send_sem=s, recv_sem=r,
            device_id=(e if ep is None else ep, t if tp is None else tp),
            device_id_type=MESH,
        )

    barrier = pltpu.get_barrier_semaphore()

    @pl.loop(1, E)
    def _(k):
        pl.semaphore_signal(barrier, inc=1, device_id=(ep_peer(k), t), device_id_type=MESH)

    for k in range(1, T):
        pl.semaphore_signal(barrier, inc=1, device_id=(e, tp_peer(k)), device_id_type=MESH)
    hf = hidden[...].astype(F32)
    inv = lax.rsqrt(jnp.mean(hf * hf, axis=-1, keepdims=True) + epsilon)
    normed = (hf * inv * mix_gain[...].reshape(1, D).astype(F32)).astype(BF16)
    for g in range(G):
        nb[g] = normed[:, 2 * g * R:2 * (g + 1) * R].reshape(2, M // 2, 2 * R)
    for p in range(E):
        ct[p] = jnp.sum(jnp.where(routes[...] == p, weights[...], 0.0), axis=0, keepdims=True)
    pl.semaphore_wait(barrier, E - 1 + T - 1)

    core = lax.rem(t, 2)

    def w_copy(i):
        return rcopy(wall.at[i, par], wall.at[i, par], w_s.at[0], w_r.at[i], ep=mate)

    def w_in(i):
        return rcopy(wall.at[i, 1 - par], wall.at[i, 1 - par], w_s.at[0], w_r.at[i], ep=mate)

    def nb_copy(g):
        return rcopy(nb.at[g, core], xin.at[g0, core], nb_s.at[0], nb_r.at[g0], ep=2 * g + par)

    def nb_in(g):
        return rcopy(nb.at[g, core], xin.at[g, core], nb_s.at[0], nb_r.at[g], ep=mate)

    def nb_beside(g):
        return rcopy(xin.at[g, core], xin.at[g, core], nf_s.at[0], nf_r.at[0], tp=beside)

    rest = pl.ds(0, G - 1)

    @pl.loop(1, E)
    def _(k):
        p = ep_peer(k)
        rcopy(ct.at[p], ctr.at[e], ct_s.at[0], ct_r.at[0], ep=p).start()

    @pl.loop(1, G)
    def _(k):
        nb_copy(peer_group(k)).start()

    pltpu.make_async_copy(wall.at[:, par], wall.at[:, par], w_l.at[0]).wait()
    for i in range(chunks):
        w_copy(i).start()

    loads[5].wait()
    loads[6].wait()
    h = dg.shape[1] // T
    half = dwp.shape[2] // 2
    if half != h:
        dwp[...] = jnp.zeros_like(dwp)
    for j in range(T):
        dwp[j, :, :h] = dg[:, j * h:(j + 1) * h]
        dwp[j, :, half:half + h] = du[:, j * h:(j + 1) * h]
    own_dw.start()
    for k in range(1, T):
        j = tp_peer(k)
        rcopy(dwp.at[j], dwr.at[t], dw_s.at[0], dw_r.at[0], tp=j).start()
    for l in loads[1:5]:
        l.start()

    xin[g0] = nb[g0]

    @pl.loop(1, G)
    def _(k):
        g = peer_group(k)
        nb_in(g).wait_recv()
        nb_beside(g).start()

    others = pl.ds(0, E - 1)
    ct_all = rcopy(ct.at[others], ctr.at[others], ct_s.at[0], ct_r.at[0], ep=mate)
    ct_all.wait_recv()

    ctr[e] = ct[e]
    for s in range(E):
        w_ref[s // 2, :, s % 2 * M:(s % 2 + 1) * M] = ctr[s]
    bd[...] = jnp.zeros_like(bd)
    block = ig.shape[1]
    width = bd.shape[1]
    per = width // block
    for i in range(ig.shape[0]):
        lo = i % per * block
        bd[i // per, lo:lo + block, lo:lo + block] = ig[i]
        bd[i // per, lo:lo + block, width + lo:width + lo + block] = dgate[i]
    def before(n):
        row = lax.broadcasted_iota(jnp.int32, (n, n), 0)
        col = lax.broadcasted_iota(jnp.int32, (n, n), 1)
        return ((row < col) & (row // M == col // M)).astype(F32).astype(BF16)

    def rank_of(m, earlier):
        rows = max(16, m.shape[0])
        return dot(jnp.broadcast_to(m, (rows, m.shape[1])).astype(BF16), earlier)[0:1]

    pair = 2 * M
    lower = before(pair)
    slot = lax.broadcasted_iota(jnp.int32, (2 * cap, pair), 0)
    first_slot = lax.broadcasted_iota(jnp.int32, (2 * cap, pair), 1) // M * cap
    slot = (slot - first_slot).astype(F32)

    @pl.loop(0, G)
    def _(g):
        w_row = w_ref[g]
        m = (w_row > 0.0).astype(F32)
        hit = (slot == rank_of(m, lower)).astype(F32) * m
        sel[g] = hit.astype(BF16)
        w_slot[g] = jnp.broadcast_to(jnp.sum(hit * w_row, axis=1, keepdims=True), w_slot.shape[1:])

    lower = before(M)
    slot = lax.broadcasted_iota(jnp.int32, (cap, M), 0).astype(F32)

    def own_hit(p):
        m = (ct[p] > 0.0).astype(F32)
        return (slot == rank_of(m, lower)).astype(F32) * m

    @pl.loop(0, G)
    def _(g):
        own_sel[g] = jnp.concatenate([own_hit(2 * g), own_hit(2 * g + 1)], axis=0).astype(BF16)

    def z_copy(i, g):
        return rcopy(zout.at[i, g], zrec.at[i, g0], pz_s.at[0], pz_r.at[i], ep=2 * g + par)

    def z_in(i):
        return rcopy(zout.at[i, rest], zrec.at[i, rest], pz_s.at[0], pz_r.at[i], ep=mate)

    nb_all = rcopy(xin.at[rest, core], xin.at[rest, core], nf_s.at[0], nf_r.at[0], tp=beside)
    nb_all.wait_recv()
    for i in range(chunks):
        w_in(i).wait_recv()
        z = dot(xin[...].reshape(G * M, 2 * R), wall[i].reshape(2 * R, CW)).reshape(G, M, CW)
        zf[...] = z
        zout[i] = z.astype(BF16)

        @pl.loop(1, G)
        def _(k):
            z_copy(i, peer_group(k)).start()

        acc[:, i * CW:(i + 1) * CW] = zf[g0]

    for i in range(chunks):
        z_in(i).wait_recv()

        @pl.loop(1, G)
        def _(k):
            g = peer_group(k)
            acc[:, i * CW:(i + 1) * CW] += zrec[i, g].astype(F32)

    x_b = acc[:, :C].astype(BF16)
    y_b = acc[:, C:].astype(BF16)
    for i in range(1, conv_old.shape[0]):
        conv_new[i - 1] = conv_old[i]
    conv_new[conv_old.shape[0] - 1] = x_b
    conv_pre = conv_old[0].astype(F32) * taps[0:1, :].astype(F32)
    for i in range(1, taps.shape[0] - 1):
        conv_pre = conv_pre + conv_old[i].astype(F32) * taps[i:i + 1, :].astype(F32)
    conv = (conv_pre + x_b.astype(F32) * taps[taps.shape[0] - 1:, :].astype(F32)).astype(BF16)
    gi, gd = [], []
    for i in range(C // width):
        g = dot(conv[:, i * width:(i + 1) * width], bd[i])
        gi.append(g[:, :width])
        gd.append(g[:, width:])
    gate_in = jax.nn.sigmoid(jnp.concatenate(gi, axis=1))
    gate_dec = jax.nn.sigmoid(jnp.concatenate(gd, axis=1))
    dp = decay_param[...]
    log_decay = decay_scale * gate_dec * (jnp.minimum(dp, 0.0) - jnp.log1p(jnp.exp(-jnp.abs(dp))))
    decay = jnp.exp(log_decay)
    inject = jnp.sqrt(-jnp.tanh(log_decay) * (1.0 + decay * decay))
    state = decay * lru[...] + inject * gate_in * conv.astype(F32)
    new_lru[...] = state
    gated = (state * jax.nn.gelu(y_b.astype(F32), approximate=True)).astype(BF16)

    loads[0].wait()
    order = [tp_peer(k) for k in (2, 3, 1)] if T == 4 else [tp_peer(k) for k in range(1, T)]
    for j in order:
        cols = pl.ds(pl.multiple_of(j * C, 128), C)
        mbuf[j] = dot(gated, po[:, cols]).astype(BF16)
        rcopy(mbuf.at[j], mrec.at[t], mx_s.at[0], mx_r.at[0], tp=j).start()
    mixer = dot(gated, po[:, own_cols]).astype(BF16).astype(F32)
    mx_all = rcopy(mbuf.at[pl.ds(0, T - 1)], mrec.at[pl.ds(0, T - 1)], mx_s.at[0], mx_r.at[0], tp=across)
    mx_all.wait_recv()
    for j in order:
        mixer = mixer + mrec[j].astype(F32)
    summed = (hidden[:, own_cols].astype(F32) + mixer).astype(BF16)
    summed_ref[...] = summed
    sf = summed.astype(F32)
    ssq = jnp.sum(sf * sf, axis=1, keepdims=True)
    same = lax.broadcasted_iota(jnp.int32, (M, M), 0) == lax.broadcasted_iota(jnp.int32, (M, M), 1)
    me = t * E + e
    srow[me] = jnp.sum(jnp.where(same, ssq, 0.0), axis=0, keepdims=True)

    def each_other(fn):
        @pl.loop(1, E * T)
        def _(k):
            r = lax.rem(e * T + t + k, E * T)
            fn(r // T, lax.rem(r, T))

    def scale_to(p, q):
        return rcopy(srow.at[me], srow.at[me], q_s.at[0], q_r.at[0], ep=p, tp=q)

    each_other(lambda p, q: scale_to(p, q).start())
    everyone = pl.ds(0, E * T - 1)
    scale_all = rcopy(srow.at[everyone], srow.at[everyone], q_s.at[0], q_r.at[0], tp=across)
    xall[me] = (sf * ffn_gain[own_cols].reshape(1, C).astype(F32)).astype(BF16)

    to_across = core * (across - t)
    to_mate = (1 - core) * (mate - e)
    first = dict(ep=e + to_mate, tp=t + to_across)
    second = dict(ep=e + core * (mate - e), tp=t + (1 - core) * (across - t))

    def slice_a(k):
        return t, 2 * peer_group(k) + par

    def slice_b(k):
        q, s = slice_a(k)
        return q + to_across, s + (1 - core) * (mate_of(s) - s)

    def slice_c(k):
        q, s = slice_a(k)
        return q + (1 - core) * (across - t), s + core * (mate_of(s) - s)

    def slice_d(k):
        q, s = slice_a(k)
        return across, mate_of(s)

    def move(at, r, **to):
        q, s = at
        return rcopy(xall.at[q * E + s], xall.at[q * E + s], x_s.at[0], r, **to)

    def landed(i, k):
        move(slice_a(k), x_r.at[i, peer_group(k)], ep=mate).wait_recv()

    def rail_a(k):
        return move(slice_a(0), x_r.at[0, g0], ep=2 * peer_group(k) + par)

    def rail_b(k):
        return move(slice_b(0), x_r.at[1, g0], ep=2 * peer_group(k) + par)

    def first_a(k):
        return move(slice_a(k), x_r.at[1, peer_group(k)], **first)

    def second_a(k):
        return move(slice_a(k), x_r.at[2, peer_group(k)], **second)

    def second_b(k):
        return move(slice_b(k), x_r.at[3, peer_group(k)], **second)

    def beside_of(i, k):
        return move((slice_a, slice_b, slice_c, slice_d)[i](k), xb_r.at[peer_group(k)], tp=beside)

    def pass_on(i, k):
        if i == 0:
            second_a(k).start()
        if i == 1:
            second_b(k).start()
        beside_of(i, k).start()

    first_a(0).start()

    @pl.loop(1, G)
    def _(k):
        rail_a(k).start()

    pass_on(0, 0)
    own_dw.wait()
    peers = pl.ds(0, T - 1)
    dw_all = rcopy(dwp.at[peers], dwr.at[peers], dw_s.at[0], dw_r.at[0], tp=across)
    dw_all.wait_recv()
    square = (
        lax.broadcasted_iota(jnp.int32, (pair, pair), 0) == lax.broadcasted_iota(jnp.int32, (pair, pair), 1)
    )

    def a_copy(q, g, r, to):
        return rcopy(aall.at[q, g], aall.at[q, g], a_s.at[0], r.at[g], tp=to)

    def pair_in(k):
        g = peer_group(k)
        for i in range(2):
            s = 2 * g + i
            total = jnp.zeros((1, M), F32)
            for q in range(T):
                total = total + srow[q * E + s]
            prow[:, i * M:(i + 1) * M] = total
        rcopy(xall.at[pl.ds(0, 4)], xall.at[pl.ds(0, 4)], x_s.at[0], xb_r.at[g], tp=beside).wait_recv()
        scale_row = lax.rsqrt(prow[...] * (1.0 / D) + epsilon)
        scale = jnp.sum(jnp.where(square, scale_row, 0.0), axis=1, keepdims=True)
        h = None
        for q in range(T):
            part = dot(xall[pl.ds(q * E + 2 * g, 2)].reshape(pair, C), dwr[q])
            h = part if h is None else h + part
        h = h * scale
        half = h.shape[1] // 2
        act = jax.nn.silu(h) * pltpu.roll(h, half, axis=1)
        aall[t, g] = act[:, :half].astype(BF16)
        a_copy(t, g, a_r, across).start()
        a_copy(t, g, ab_r, beside).start()
        pick = sel[g]
        for q in range(T):
            xe[g, :, q * C:(q + 1) * C] = dot(pick, xall[pl.ds(q * E + 2 * g, 2)].reshape(pair, C)).astype(BF16)
        s_slot[g] = jnp.broadcast_to(
            jnp.sum(pick.astype(F32) * scale_row, axis=1, keepdims=True), s_slot.shape[1:]
        )

    def a_forward(k):
        g = peer_group(k)
        a_copy(across, g, a_r, across).wait_recv()
        a_copy(across, g, ab_r, beside).start()

    gate = jax.nn.sigmoid(branch[...])

    def dense(k):
        g = peer_group(k)
        rcopy(aall.at[pl.ds(0, 2), g], aall.at[pl.ds(0, 2), g], a_s.at[0], ab_r.at[g], tp=beside).wait_recv()
        d = dot(aall[0, g], dd[0])
        for q in range(1, T):
            d = d + dot(aall[q, g], dd[q])
        dtmp[...] = (d * gate).reshape(2, M, C)
        om[g] = dtmp[1 - par].astype(BF16)
        rcopy(om.at[g], orm.at[g], om_s.at[0], om_r.at[g], ep=mate).start()
        dacc[g] = dtmp[par]

    def dense_on(k):
        g = peer_group(k)
        rcopy(om.at[g], orm.at[g], om_s.at[0], om_r.at[g], ep=mate).wait_recv()
        oz[g] = (dacc[g] + orm[g].astype(F32)).astype(BF16)
        rcopy(oz.at[g], ozr.at[g0], oz_s.at[0], oz_r.at[0], ep=2 * g + par).start()

    for l in loads[4:5]:
        l.wait()

    lag = 2

    @pl.loop(0, G + lag)
    def _(k):
        @pl.when((k >= 1) & (k < G))
        def _():
            landed(0, k)

            @pl.when(core == 0)
            def _():
                first_a(k).start()

            pass_on(0, k)

        @pl.when((k >= 1) & (k <= G))
        def _():
            landed(1, k - 1)

            @pl.when((core == 1) & (k == 1))
            def _():
                @pl.loop(1, G)
                def _(j):
                    rail_b(j).start()

            pass_on(1, k - 1)
            landed(2, k - 1)
            pass_on(2, k - 1)

        @pl.when((k >= 2) & (k <= G + 1))
        def _():
            landed(3, k - 2)
            pass_on(3, k - 2)

        @pl.when(k == lag)
        def _():
            scale_all.wait_recv()

        @pl.when(k >= lag)
        def _():
            pair_in(k - lag)

        @pl.when(k >= lag + 1)
        def _():
            a_forward(k - lag - 1)

        @pl.when(k >= lag + 2)
        def _():
            dense(k - lag - 2)

        @pl.when(k >= lag + 4)
        def _():
            dense_on(k - lag - 3)

    loads[1].wait()
    loads[2].wait()
    FH = eg.shape[1]
    nch = 256 if FH % 256 == 0 else FH
    slots = E * cap

    @pl.loop(0, FH // nch)
    def _(n):
        cols = pl.ds(pl.multiple_of(n * nch, 128), nch)
        rows_in = xe[...].reshape(slots, D)
        scale = s_slot[...].reshape(slots, 128)[:, 0:1]
        g = dot(rows_in, eg[:, cols]) * scale
        u = dot(rows_in, eu[:, cols]) * scale
        hid[:, cols] = (jax.nn.silu(g) * u).astype(BF16)

    loads[3].wait()

    def down(j):
        return dot(hid[...], ed[:, pl.ds(pl.multiple_of(j * C, 128), C)])

    def e_copy(i):
        return rcopy(ebuf.at[i], erec.at[i], ed_s.at[0], ed_r.at[i], tp=beside)

    def ex_copy(g):
        return rcopy(ex.at[g], exr.at[g], ex_s.at[0], ex_r.at[g], tp=across)

    def eo_copy(s, p):
        return rcopy(eo.at[s], eor.at[p], eo_s.at[0], eo_r.at[0], ep=s)

    def ex_out(k):
        g = peer_group(k)
        ex[g] = (epart[1, g] + erec[1, g].astype(F32)).astype(BF16)
        ex_copy(g).start()

    def ex_in(k):
        g = peer_group(k)
        ex_copy(g).wait_recv()
        red = epart[0, g] + erec[0, g].astype(F32) + exr[g].astype(F32)
        red = red.astype(BF16).astype(F32) * w_slot[g][:, 0:1]
        eo[pl.ds(2 * g, 2)] = red.reshape(2, cap, C).astype(BF16)
        for i in range(2):
            s = 2 * g + i

            @pl.when(s != e)
            def _():
                eo_copy(s, e).start()

    for i, j in ((1, diagonal), (0, beside)):
        ebuf[i] = down(j).reshape(G, 2 * cap, C).astype(BF16)
        e_copy(i).start()
    a_forward(G - 1)
    epart[1] = down(across).reshape(G, 2 * cap, C)
    epart[0] = down(t).reshape(G, 2 * cap, C)
    e_copy(1).wait_recv()

    @pl.loop(0, G)
    def _(k):
        ex_out(G - 1 - k)

    if G > 1:
        dense(G - 2)
    if G > 3:
        dense_on(G - 3)
    dense(G - 1)
    if G > 2:
        dense_on(G - 2)
    e_copy(0).wait_recv()
    ex_in(G - 1)
    if G > 1:
        dense_on(G - 1)

    @pl.loop(1, G)
    def _(k):
        ex_in(G - 1 - k)

    eor[e] = eo[e]
    rcopy(om.at[g0], orm.at[g0], om_s.at[0], om_r.at[g0], ep=mate).wait_recv()
    acc[:, :C] = summed_ref[...].astype(F32) + dacc[g0] + orm[g0].astype(F32)

    oz_all = rcopy(oz.at[rest], ozr.at[rest], oz_s.at[0], oz_r.at[0], ep=mate)
    oz_all.wait_recv()

    @pl.loop(1, G)
    def _(k):
        g = peer_group(k)
        acc[:, :C] += ozr[g].astype(F32)


    eo_all = rcopy(eo.at[others], eor.at[others], eo_s.at[0], eo_r.at[0], ep=mate)
    eo_all.wait_recv()

    picked = eor[...].astype(F32).reshape(slots, C).astype(BF16)
    new_hidden[...] = (
        acc[:, :C] + lax.dot_general(
            own_sel[...].reshape(slots, M), picked, (((0,), (0,)), ((), ())), preferred_element_type=F32
        )
    ).astype(BF16)
    for copy in (ct_all, nb_all, dw_all, mx_all, scale_all, oz_all, eo_all):
        copy.wait_send()
    z_all = zout.at[:, rest]
    for ref, sem in (
        (wall.at[:, par], w_s), (nb.at[rest, core], nb_s), (z_all, pz_s), (xall.at[everyone], x_s),
        (aall.at[pl.ds(0, 3)], a_s), (ebuf, ed_s), (ex, ex_s), (om, om_s),
    ):
        rcopy(ref, ref, sem.at[0], sem.at[0], tp=across).wait_send()


def store_kernel(a, b, c, a_out, b_out, c_out, sems):
    copies = [
        pltpu.make_async_copy(src, dst, sems.at[i])
        for i, (src, dst) in enumerate(((a, a_out), (b, b_out), (c, c_out)))
    ]
    for copy in copies:
        copy.start()
    for copy in copies:
        copy.wait()


def on_device(
    hidden, mix_gain, proj_x, proj_y, conv_taps, input_gate, decay_gate, decay_param,
    proj_out, conv_state, lru_state, ffn_gain, routes, route_weights,
    expert_gate, expert_up, expert_down, dense_gate, dense_up, dense_down, branch_gate,
):
    E = lax.axis_size("ep")
    T = lax.axis_size("tp")
    M, D = hidden.shape
    C = D // T
    R = proj_x.shape[0]
    N = E * M
    heads, block = input_gate.shape[:2]
    group = max(1, 128 // block)

    experts = expert_gate.shape[0] * E
    cap = -(-(M * routes.shape[1] // experts + 2) // 8) * 8
    slots = E * cap
    G = E // 2
    h = dense_gate.shape[1] // T
    half = -(-2 * h // 128) * 64

    dd = jnp.pad(dense_down.reshape(T, h, C), ((0, 0), (0, half - h), (0, 0)))
    FH = expert_gate.shape[2]
    vm = pl.BlockSpec(memory_space=pltpu.VMEM)
    anyspace = pl.BlockSpec(memory_space=pl.ANY)
    DMA = pltpu.SemaphoreType.DMA
    V = pltpu.VMEM
    chunks = max(1, 2 * C // 128)
    scratch = [
        V((E, 1, M), F32), V((G, 1, 2 * M), F32), V((heads // group, group * block, 2 * group * block), BF16),
        V((chunks, 2, R, 2 * C // chunks), BF16), V((C, T * h), BF16), V((C, T * h), BF16),
        V((C, D), BF16), V((D, FH), BF16), V((D, FH), BF16), V((FH, D), BF16), V((T, half, C), BF16),
        V((G, 2, M // 2, 2 * R), BF16), V((T, C, 2 * half), BF16), V((T, C, 2 * half), BF16),
        V((G, 2, M // 2, 2 * R), BF16), V((G, M, 2 * C // chunks), F32),
        V((chunks, G, M, 2 * C // chunks), BF16), V((chunks, G, M, 2 * C // chunks), BF16),
        V((E, 1, M), F32), V((M, 2 * C), F32),
        V((T, M, C), BF16), V((T, M, C), BF16), V((T * E, 1, M), F32), V((1, 2 * M), F32),
        V((T * E, M, C), BF16), V((T, G, 2 * M, half), BF16),
        V((G, 2 * cap, D), BF16), V((slots, FH), BF16), V((G, 2 * cap, 2 * M), BF16),
        V((G, 2 * cap, M), BF16), V((G, 2 * cap, 128), F32), V((G, 2 * cap, 128), F32),
        V((2, G, 2 * cap, C), BF16), V((2, G, 2 * cap, C), BF16), V((2, G, 2 * cap, C), F32),
        V((G, 2 * cap, C), BF16), V((G, 2 * cap, C), BF16), V((E, cap, C), BF16), V((E, cap, C), BF16),
        V((2, M, C), F32),
        V((G, M, C), BF16), V((G, M, C), F32), V((G, M, C), BF16), V((G, M, C), BF16), V((G, M, C), BF16),
        V((M, C), BF16),
        DMA((8,)), DMA((1,)), DMA((1,)), DMA((chunks,)),
        DMA((1,)), DMA((G,)), DMA((1,)), DMA((1,)), DMA((1,)), DMA((1,)), DMA((1,)), DMA((chunks,)),
        DMA((1,)), DMA((1,)), DMA((1,)), DMA((1,)), DMA((1,)), DMA((1,)),
        DMA((1,)), DMA((4, G)), DMA((G,)), DMA((1,)), DMA((G,)), DMA((G,)),
        DMA((1,)), DMA((2,)), DMA((1,)), DMA((G,)), DMA((1,)), DMA((1,)),
        DMA((1,)), DMA((G,)), DMA((1,)), DMA((1,)),
    ]
    outs = pl.pallas_call(
        functools.partial(layer_kernel, E, T, cap),
        out_shape=(V((M, C), BF16), V((M, C), F32), V((conv_state.shape[1], M, C), BF16)),
        in_specs=[vm] * 12 + [anyspace] * 9,
        out_specs=(vm, vm, vm),
        scratch_shapes=scratch,
        compiler_params=pltpu.CompilerParams(
            collective_id=0, has_side_effects=True, vmem_limit_bytes=60 * 1024 * 1024
        ),
    )(
        hidden, mix_gain, routes.T, route_weights.T, conv_state.transpose(1, 0, 2), conv_taps,
        input_gate, decay_gate, decay_param[None, :], lru_state,
        ffn_gain, branch_gate[None, :],
        proj_x, proj_y, dense_gate, dense_up, proj_out, expert_gate[0], expert_up[0], expert_down[0], dd,
    )
    new_hidden, new_lru, new_conv = pl.pallas_call(
        store_kernel,
        out_shape=tuple(jax.ShapeDtypeStruct(o.shape, o.dtype) for o in outs),
        in_specs=[vm] * 3,
        out_specs=(anyspace,) * 3,
        scratch_shapes=[DMA((3,))],
    )(*(pltpu.with_memory_space_constraint(o, pltpu.VMEM) for o in outs))
    return (new_hidden, new_lru, new_conv.transpose(1, 0, 2))


def solution(mesh):
    in_specs = (
        P("ep", None),
        P(),
        P("ep", "tp"),
        P("ep", "tp"),
        P(None, "tp"),
        P("tp", None, None),
        P("tp", None, None),
        P("tp"),
        P("tp", None),
        P("ep", None, "tp"),
        P("ep", "tp"),
        P(),
        P("ep", None),
        P("ep", None),
        P("ep", None, "tp"),
        P("ep", None, "tp"),
        P("ep", "tp", None),
        P("tp", "ep"),
        P("tp", "ep"),
        P("ep", "tp"),
        P("tp"),
    )
    out_specs = (P("ep", "tp"), P("ep", "tp"), P("ep", None, "tp"))
    return jax.shard_map(
        on_device, mesh=mesh, in_specs=in_specs, out_specs=out_specs, check_vma=False
    )
```

time: 82.8 us -> 71.6 us (0.86)
  Pallas kernels: 82 us -> 70.8 us
    pallas_call x1, Pallas kernels: 80.2 us -> 70.1 us  [on_device(): pl.pallas_call(functools.partial(layer_kernel, E, T, cap), out_shape=(V((...]
    pallas_call x1, Pallas kernels: 1.79 us -> 0.77 us  [on_device(): pl.pallas_call(store_kernel, out_shape=tuple((jax.ShapeDtypeStruct(o.shap...]
where the time goes in v2:
time: 71.6 us; the launch traced here: 71.5 us
  Pallas kernels  70.8 us (99%)
    pallas_call x1, Pallas kernels, on_device(): pl.pallas_call(functools.partial(layer_kernel, E, T, cap), out_shape=(V((...  70.1 us

profile of v2, /device:TPU:0, one launch (start us, length us, event | category | flops | bytes accessed | tf_op | source)
XLA Modules:
  0.0 71.5 jit_solution(14468098109862039760)
XLA Ops:
  0.6 70.1 %shard_map.220 = (bf16[64,512]{1,0:T(8,128)(2,1)S(1)}, f32[64,512]{1,0:T(8,128)S(1)}, bf16[3,64,512]{2,1,0:T(8,128)(2,1)S(1)}) custom-call(bf16[64,2048]{1,0:T(8,128)(2,1)} %hidden.1, bf16[2048]{0:T(1024)(128)(2,1)} %mix_gain.1, s32[2,64]{1,0:T(2,128)} %bitcast.17, f32[2,64]{1,0:T(2,128)} %bitcast.18, bf16[3,64,512]{2,1,0:T(8,128)(2,1)} %bitcast.14, ...), custom_call_target="tpu_custom_call" | custom-call | tf_op jit(solution)/shard_map/pallas_call | solution.py:655
  70.7 0.8 %shard_map.221 = (bf16[64,512]{1,0:T(8,128)(2,1)}, f32[64,512]{1,0:T(8,128)}, bf16[3,64,512]{2,1,0:T(8,128)(2,1)}) custom-call(bf16[64,512]{1,0:T(8,128)(2,1)S(1)} %get-tuple-element.9.a, f32[64,512]{1,0:T(8,128)S(1)} %get-tuple-element.10.b, bf16[3,64,512]{2,1,0:T(8,128)(2,1)S(1)} %get-tuple-element.11.c), custom_call_target="tpu_custom_call" | custom-call | tf_op jit(solution)/shard_map/pallas_call | solution.py:670

commit v3 on v2

--- a/solution.py
+++ b/solution.py
@@ -10,6 +10,7 @@
 epsilon = 1e-06
 decay_scale = 8.0
 MESH = pl.DeviceIdType.MESH
+DIRECT = 3
 F32 = jnp.float32
 BF16 = jnp.bfloat16
 
@@ -20,14 +21,16 @@
 
 def layer_kernel(
     E, T, cap,
-    hidden, mix_gain, routes, weights, conv_old, taps, ig, dgate, decay_param, lru, ffn_gain, branch,
+    hidden_h, mix_gain_h, routes_h, weights_h, conv_old_h, taps_h, ig_h, dgate_h, decay_param_h, lru_h,
+    ffn_gain_h, branch_h,
     wx_h, wy_h, dg_h, du_h, po_h, eg_h, eu_h, ed_h, dd_h,
     new_hidden, new_lru, conv_new,
-    ct, w_ref, bd, wall, dg, du, po, eg, eu, ed, dd, nb, dwp, dwr, xin, zf, zout, zrec, ctr, acc,
-    mbuf, mrec, srow, prow, xall, aall, xe, hid, sel, own_sel, w_slot, s_slot,
-    ebuf, erec, epart, ex, exr, eo, eor, dtmp, om, dacc, orm, oz, ozr, summed_ref,
-    load_sem, w_l, w_s, w_r, nb_s, nb_r, nf_s, nf_r, ct_s, ct_r, pz_s, pz_r, dw_s, dw_r, mx_s, mx_r, q_s, q_r,
-    x_s, x_r, xb_r, a_s, a_r, ab_r, ed_s, ed_r, ex_s, ex_r, eo_s, eo_r, om_s, om_r, oz_s, oz_r,
+    hidden, mix_gain, routes, weights, conv_old, taps, ig, dgate, decay_param, lru, ffn_gain, branch,
+    ct, w_ref, bd, wall, dg, du, po, eg, eu, ed, dd, nb, dwp, dwr, xin, zf, zlast, zpair, zout, zrec, ctr, acc,
+    mbuf, mrec, srow, stot, prow, xall, aall, xe, hid, sel, own_sel, w_slot, s_slot,
+    ebuf, erec, epart, ex, exr, eo, eor, dtmp, om, dacc, orm, oz, ozr, ozx, summed_ref,
+    load_sem, in_l, w_l, w_s, w_r, nb_s, nb_r, nf_s, nf_r, ct_s, ct_r, pz_s, pz_r, zx_r, dw_s, dw_r, mx_s, mx_r, q_s, q_r, qe_s, qe_r,
+    x_s, x_r, xb_r, a_s, a_r, ab_r, ed_s, ed_r, ex_s, ex_r, eo_s, eo_r, om_s, om_r, oz_s, oz_r, ozx_r, ozf_r,
 ):
     e = lax.axis_index("ep")
     t = lax.axis_index("tp")
@@ -56,14 +59,20 @@
     def mate_of(s):
         return s + 1 - 2 * lax.rem(s, 2)
 
+    upper = G // 2
+    paired = G > 2 and G & (G - 1) == 0
+
+    def flip(g, mask):
+        out, bit = 0, 1
+        while bit < G:
+            out = out + bit * lax.rem(g // bit + mask // bit, 2)
+            bit *= 2
+        return out
+
     def peer_group(k):
-        if G & (G - 1):
+        if not paired:
             return lax.rem(g0 + k, G)
-        g, bit = 0, 1
-        while bit < G:
-            g = g + bit * lax.rem(g0 // bit + k // bit, 2)
-            bit *= 2
-        return g
+        return flip(g0, k // upper * upper + lax.rem(k + k // upper, upper))
 
     def tp_peer(k):
         return lax.rem(t + k, T)
@@ -71,6 +80,26 @@
     across = lax.rem(t + T // 2, T)
     beside = t + 1 - 2 * lax.rem(t, 2)
     diagonal = lax.rem(beside + T // 2, T)
+
+    inputs = [
+        pltpu.make_async_copy(src, dst, in_l.at[i])
+        for i, (src, dst) in enumerate(
+            ((hidden_h, hidden), (mix_gain_h, mix_gain), (routes_h, routes), (weights_h, weights),
+             (conv_old_h, conv_old), (taps_h, taps), (ig_h, ig), (dgate_h, dgate),
+             (decay_param_h, decay_param), (lru_h, lru), (ffn_gain_h, ffn_gain), (branch_h, branch))
+        )
+    ]
+    for copy in inputs[:4]:
+        copy.start()
+
+    barrier = pltpu.get_barrier_semaphore()
+
+    @pl.loop(1, E)
+    def _(k):
+        pl.semaphore_signal(barrier, inc=1, device_id=(ep_peer(k), t), device_id_type=MESH)
+
+    for k in range(1, T):
+        pl.semaphore_signal(barrier, inc=1, device_id=(e, tp_peer(k)), device_id_type=MESH)
 
     loads = [
         pltpu.make_async_copy(src, dst, load_sem.at[i])
@@ -89,6 +118,8 @@
         w_load(i).start()
     for i in (5, 6, 0):
         loads[i].start()
+    for copy in inputs[4:]:
+        copy.start()
 
     def rcopy(src, dst, s, r, ep=None, tp=None):
         return pltpu.make_async_remote_copy(
@@ -97,14 +128,8 @@
             device_id_type=MESH,
         )
 
-    barrier = pltpu.get_barrier_semaphore()
-
-    @pl.loop(1, E)
-    def _(k):
-        pl.semaphore_signal(barrier, inc=1, device_id=(ep_peer(k), t), device_id_type=MESH)
-
-    for k in range(1, T):
-        pl.semaphore_signal(barrier, inc=1, device_id=(e, tp_peer(k)), device_id_type=MESH)
+    for copy in inputs[:4]:
+        copy.wait()
     hf = hidden[...].astype(F32)
     inv = lax.rsqrt(jnp.mean(hf * hf, axis=-1, keepdims=True) + epsilon)
     normed = (hf * inv * mix_gain[...].reshape(1, D).astype(F32)).astype(BF16)
@@ -162,6 +187,8 @@
     for l in loads[1:5]:
         l.start()
 
+    for copy in inputs[4:]:
+        copy.wait()
     xin[g0] = nb[g0]
 
     @pl.loop(1, G)
@@ -219,11 +246,24 @@
     def _(g):
         own_sel[g] = jnp.concatenate([own_hit(2 * g), own_hit(2 * g + 1)], axis=0).astype(BF16)
 
+    early = max(0, chunks - DIRECT) if paired else 0
+    last = flip(g0, upper)
+
     def z_copy(i, g):
         return rcopy(zout.at[i, g], zrec.at[i, g0], pz_s.at[0], pz_r.at[i], ep=2 * g + par)
 
     def z_in(i):
-        return rcopy(zout.at[i, rest], zrec.at[i, rest], pz_s.at[0], pz_r.at[i], ep=mate)
+        some = pl.ds(0, upper if i < early else G - 1)
+        return rcopy(zout.at[i, some], zrec.at[i, some], pz_s.at[0], pz_r.at[i], ep=mate)
+
+    def z_pair(i):
+        some = pl.ds(0, upper - 1)
+        rcopy(zout.at[i, some], zpair.at[i, some], pz_s.at[0], zx_r.at[i], ep=mate).wait_recv()
+        total = zlast[i]
+        for low in range(1, upper):
+            total = total + zpair[i, flip(g0, low)].astype(F32)
+        zout[i, last] = total.astype(BF16)
+        z_copy(i, last).start()
 
     nb_all = rcopy(xin.at[rest, core], xin.at[rest, core], nf_s.at[0], nf_r.at[0], tp=beside)
     nb_all.wait_recv()
@@ -233,18 +273,31 @@
         zf[...] = z
         zout[i] = z.astype(BF16)
 
-        @pl.loop(1, G)
-        def _(k):
-            z_copy(i, peer_group(k)).start()
+        if i < early:
+            for low in range(1, upper):
+                to = flip(g0, low)
+                g = flip(to, upper)
+                rcopy(zout.at[i, g], zpair.at[i, g0], pz_s.at[0], zx_r.at[i], ep=2 * to + par).start()
+                z_copy(i, to).start()
+            zlast[i] = zf[last]
+        else:
+            @pl.loop(1, G)
+            def _(k):
+                z_copy(i, peer_group(k)).start()
 
         acc[:, i * CW:(i + 1) * CW] = zf[g0]
+        if 0 <= i - 2 < early:
+            z_pair(i - 2)
+
+    for i in range(max(0, chunks - 2), early):
+        z_pair(i)
 
     for i in range(chunks):
         z_in(i).wait_recv()
 
-        @pl.loop(1, G)
+        @pl.loop(0 if i < early else 1, upper if i < early else G)
         def _(k):
-            g = peer_group(k)
+            g = flip(g0, k + 1) if i < early else peer_group(k)
             acc[:, i * CW:(i + 1) * CW] += zrec[i, g].astype(F32)
 
     x_b = acc[:, :C].astype(BF16)
@@ -288,20 +341,11 @@
     ssq = jnp.sum(sf * sf, axis=1, keepdims=True)
     same = lax.broadcasted_iota(jnp.int32, (M, M), 0) == lax.broadcasted_iota(jnp.int32, (M, M), 1)
     me = t * E + e
-    srow[me] = jnp.sum(jnp.where(same, ssq, 0.0), axis=0, keepdims=True)
-
-    def each_other(fn):
-        @pl.loop(1, E * T)
-        def _(k):
-            r = lax.rem(e * T + t + k, E * T)
-            fn(r // T, lax.rem(r, T))
-
-    def scale_to(p, q):
-        return rcopy(srow.at[me], srow.at[me], q_s.at[0], q_r.at[0], ep=p, tp=q)
-
-    each_other(lambda p, q: scale_to(p, q).start())
+    ssq_row = jnp.sum(jnp.where(same, ssq, 0.0), axis=0, keepdims=True)
+    srow[t] = ssq_row
+    ssq_all = rcopy(srow.at[pl.ds(0, T - 1)], srow.at[pl.ds(0, T - 1)], q_s.at[0], q_r.at[0], tp=across)
+    scale_all = rcopy(stot.at[others], stot.at[others], qe_s.at[0], qe_r.at[0], ep=mate)
     everyone = pl.ds(0, E * T - 1)
-    scale_all = rcopy(srow.at[everyone], srow.at[everyone], q_s.at[0], q_r.at[0], tp=across)
     xall[me] = (sf * ffn_gain[own_cols].reshape(1, C).astype(F32)).astype(BF16)
 
     to_across = core * (across - t)
@@ -363,6 +407,8 @@
         rail_a(k).start()
 
     pass_on(0, 0)
+    for j in order:
+        rcopy(srow.at[t], srow.at[t], q_s.at[0], q_r.at[0], tp=j).start()
     own_dw.wait()
     peers = pl.ds(0, T - 1)
     dw_all = rcopy(dwp.at[peers], dwr.at[peers], dw_s.at[0], dw_r.at[0], tp=across)
@@ -377,11 +423,7 @@
     def pair_in(k):
         g = peer_group(k)
         for i in range(2):
-            s = 2 * g + i
-            total = jnp.zeros((1, M), F32)
-            for q in range(T):
-                total = total + srow[q * E + s]
-            prow[:, i * M:(i + 1) * M] = total
+            prow[:, i * M:(i + 1) * M] = stot[2 * g + i]
         rcopy(xall.at[pl.ds(0, 4)], xall.at[pl.ds(0, 4)], x_s.at[0], xb_r.at[g], tp=beside).wait_recv()
         scale_row = lax.rsqrt(prow[...] * (1.0 / D) + epsilon)
         scale = jnp.sum(jnp.where(square, scale_row, 0.0), axis=1, keepdims=True)
@@ -423,64 +465,95 @@
     def dense_on(k):
         g = peer_group(k)
         rcopy(om.at[g], orm.at[g], om_s.at[0], om_r.at[g], ep=mate).wait_recv()
-        oz[g] = (dacc[g] + orm[g].astype(F32)).astype(BF16)
-        rcopy(oz.at[g], ozr.at[g0], oz_s.at[0], oz_r.at[0], ep=2 * g + par).start()
+        total = dacc[g] + orm[g].astype(F32)
+        if paired and k == G - 1:
+            oz_pair.wait_recv()
+            for low in range(1, upper):
+                total = total + ozx[flip(g0, low)].astype(F32)
+        oz[g] = total.astype(BF16)
+        if paired and upper <= k < G - 1:
+            to = flip(g0, k - upper + 1)
+            rcopy(oz.at[g], ozx.at[g0], oz_s.at[0], ozx_r.at[0], ep=2 * to + par).start()
+        elif paired and k == G - 1:
+            rcopy(oz.at[g], ozr.at[g0], oz_s.at[0], ozf_r.at[0], ep=2 * g + par).start()
+        else:
+            rcopy(oz.at[g], ozr.at[g0], oz_s.at[0], oz_r.at[0], ep=2 * g + par).start()
+
+    direct = pl.ds(0, (upper if paired else G) - 1)
+    oz_all = rcopy(oz.at[direct], ozr.at[direct], oz_s.at[0], oz_r.at[0], ep=mate)
+    if paired:
+        oz_pair = rcopy(oz.at[direct], ozx.at[direct], oz_s.at[0], ozx_r.at[0], ep=mate)
 
     for l in loads[4:5]:
         l.wait()
 
-    lag = 2
-
-    @pl.loop(0, G + lag)
-    def _(k):
-        @pl.when((k >= 1) & (k < G))
-        def _():
-            landed(0, k)
-
-            @pl.when(core == 0)
-            def _():
-                first_a(k).start()
-
-            pass_on(0, k)
-
-        @pl.when((k >= 1) & (k <= G))
-        def _():
-            landed(1, k - 1)
-
-            @pl.when((core == 1) & (k == 1))
-            def _():
-                @pl.loop(1, G)
-                def _(j):
-                    rail_b(j).start()
-
-            pass_on(1, k - 1)
+    def a_in(k):
+        landed(0, k)
+
+        @pl.when(core == 0)
+        def _():
+            first_a(k).start()
+
+        pass_on(0, k)
+
+    landed(1, 0)
+
+    @pl.when(core == 1)
+    def _():
+        @pl.loop(1, G)
+        def _(j):
+            rail_b(j).start()
+
+    pass_on(1, 0)
+    if G > 1:
+        a_in(1)
+    ssq_all.wait_recv()
+    total = srow[0]
+    for q in range(1, T):
+        total = total + srow[q]
+    stot[e] = total
+
+    @pl.loop(1, E)
+    def _(k):
+        rcopy(stot.at[e], stot.at[e], qe_s.at[0], qe_r.at[0], ep=ep_peer(k)).start()
+
+
+    @pl.loop(1, G + 2)
+    def _(k):
+        @pl.when(k + 1 < G)
+        def _():
+            a_in(k + 1)
+
+        @pl.when(k <= G)
+        def _():
             landed(2, k - 1)
             pass_on(2, k - 1)
 
-        @pl.when((k >= 2) & (k <= G + 1))
-        def _():
-            landed(3, k - 2)
-            pass_on(3, k - 2)
-
-        @pl.when(k == lag)
+        @pl.when(k < G)
+        def _():
+            landed(1, k)
+            pass_on(1, k)
+
+        @pl.when(k <= G)
+        def _():
+            landed(3, k - 1)
+            pass_on(3, k - 1)
+
+        @pl.when(k == 2)
         def _():
             scale_all.wait_recv()
 
-        @pl.when(k >= lag)
-        def _():
-            pair_in(k - lag)
-
-        @pl.when(k >= lag + 1)
-        def _():
-            a_forward(k - lag - 1)
-
-        @pl.when(k >= lag + 2)
-        def _():
-            dense(k - lag - 2)
-
-        @pl.when(k >= lag + 4)
-        def _():
-            dense_on(k - lag - 3)
+        @pl.when(k >= 2)
+        def _():
+            pair_in(k - 2)
+
+        @pl.when(k >= 4)
+        def _():
+            a_forward(k - 4)
+
+        @pl.when(k >= 6)
+        def _():
+            dense(k - 6)
 
     loads[1].wait()
     loads[2].wait()
@@ -488,15 +561,26 @@
     nch = 256 if FH % 256 == 0 else FH
     slots = E * cap
 
-    @pl.loop(0, FH // nch)
-    def _(n):
-        cols = pl.ds(pl.multiple_of(n * nch, 128), nch)
+    def hidden_units(n):
+        cols = slice(n * nch, (n + 1) * nch)
         rows_in = xe[...].reshape(slots, D)
         scale = s_slot[...].reshape(slots, 128)[:, 0:1]
         g = dot(rows_in, eg[:, cols]) * scale
         u = dot(rows_in, eu[:, cols]) * scale
         hid[:, cols] = (jax.nn.silu(g) * u).astype(BF16)
 
+    if G < 2:
+        a_forward(0)
+    hidden_units(0)
+    if G > 3:
+        dense(G - 4)
+    for n in range(1, FH // nch):
+        hidden_units(n)
+        if n == 1:
+            if G > 1:
+                a_forward(G - 2)
+            if G > 2:
+                dense(G - 3)
     loads[3].wait()
 
     def down(j):
@@ -532,7 +616,9 @@
     for i, j in ((1, diagonal), (0, beside)):
         ebuf[i] = down(j).reshape(G, 2 * cap, C).astype(BF16)
         e_copy(i).start()
-    a_forward(G - 1)
+    if G > 1:
+        a_forward(G - 1)
+        dense(G - 2)
     epart[1] = down(across).reshape(G, 2 * cap, C)
     epart[0] = down(t).reshape(G, 2 * cap, C)
     e_copy(1).wait_recv()
@@ -541,33 +627,31 @@
     def _(k):
         ex_out(G - 1 - k)
 
-    if G > 1:
-        dense(G - 2)
-    if G > 3:
-        dense_on(G - 3)
     dense(G - 1)
-    if G > 2:
-        dense_on(G - 2)
+    for k in range(1, G - 1):
+        dense_on(k)
     e_copy(0).wait_recv()
-    ex_in(G - 1)
+
+    @pl.loop(0, G - 1)
+    def _(k):
+        ex_in(G - 1 - k)
+
     if G > 1:
         dense_on(G - 1)
-
-    @pl.loop(1, G)
-    def _(k):
-        ex_in(G - 1 - k)
-
+    ex_in(0)
     eor[e] = eo[e]
     rcopy(om.at[g0], orm.at[g0], om_s.at[0], om_r.at[g0], ep=mate).wait_recv()
     acc[:, :C] = summed_ref[...].astype(F32) + dacc[g0] + orm[g0].astype(F32)
 
-    oz_all = rcopy(oz.at[rest], ozr.at[rest], oz_s.at[0], oz_r.at[0], ep=mate)
     oz_all.wait_recv()
-
-    @pl.loop(1, G)
-    def _(k):
-        g = peer_group(k)
-        acc[:, :C] += ozr[g].astype(F32)
+    if paired:
+        oz_last = rcopy(oz.at[g0], ozr.at[g0], oz_s.at[0], ozf_r.at[0], ep=mate)
+        oz_last.wait_recv()
+        for mask in (*range(1, upper), upper):
+            acc[:, :C] += ozr[flip(g0, mask)].astype(F32)
+    else:
+        for k in range(1, G):
+            acc[:, :C] += ozr[peer_group(k)].astype(F32)
 
 
     eo_all = rcopy(eo.at[others], eor.at[others], eo_s.at[0], eo_r.at[0], ep=mate)
@@ -579,12 +663,12 @@
             own_sel[...].reshape(slots, M), picked, (((0,), (0,)), ((), ())), preferred_element_type=F32
         )
     ).astype(BF16)
-    for copy in (ct_all, nb_all, dw_all, mx_all, scale_all, oz_all, eo_all):
+    for copy in (ct_all, nb_all, dw_all, mx_all, ssq_all, scale_all, eo_all):
         copy.wait_send()
     z_all = zout.at[:, rest]
     for ref, sem in (
         (wall.at[:, par], w_s), (nb.at[rest, core], nb_s), (z_all, pz_s), (xall.at[everyone], x_s),
-        (aall.at[pl.ds(0, 3)], a_s), (ebuf, ed_s), (ex, ex_s), (om, om_s),
+        (aall.at[pl.ds(0, 3)], a_s), (ebuf, ed_s), (ex, ex_s), (om, om_s), (oz.at[rest], oz_s),
     ):
         rcopy(ref, ref, sem.at[0], sem.at[0], tp=across).wait_send()
 
@@ -628,15 +712,22 @@
     DMA = pltpu.SemaphoreType.DMA
     V = pltpu.VMEM
     chunks = max(1, 2 * C // 128)
+    small = (
+        hidden, mix_gain, routes.T, route_weights.T, conv_state.transpose(1, 0, 2), conv_taps,
+        input_gate, decay_gate, decay_param[None, :], lru_state,
+        ffn_gain, branch_gate[None, :],
+    )
     scratch = [
+        *(V(a.shape, a.dtype) for a in small),
         V((E, 1, M), F32), V((G, 1, 2 * M), F32), V((heads // group, group * block, 2 * group * block), BF16),
         V((chunks, 2, R, 2 * C // chunks), BF16), V((C, T * h), BF16), V((C, T * h), BF16),
         V((C, D), BF16), V((D, FH), BF16), V((D, FH), BF16), V((FH, D), BF16), V((T, half, C), BF16),
         V((G, 2, M // 2, 2 * R), BF16), V((T, C, 2 * half), BF16), V((T, C, 2 * half), BF16),
-        V((G, 2, M // 2, 2 * R), BF16), V((G, M, 2 * C // chunks), F32),
+        V((G, 2, M // 2, 2 * R), BF16), V((G, M, 2 * C // chunks), F32), V((chunks, M, 2 * C // chunks), F32),
+        V((chunks, G, M, 2 * C // chunks), BF16),
         V((chunks, G, M, 2 * C // chunks), BF16), V((chunks, G, M, 2 * C // chunks), BF16),
         V((E, 1, M), F32), V((M, 2 * C), F32),
-        V((T, M, C), BF16), V((T, M, C), BF16), V((T * E, 1, M), F32), V((1, 2 * M), F32),
+        V((T, M, C), BF16), V((T, M, C), BF16), V((T, 1, M), F32), V((E, 1, M), F32), V((1, 2 * M), F32),
         V((T * E, M, C), BF16), V((T, G, 2 * M, half), BF16),
         V((G, 2 * cap, D), BF16), V((slots, FH), BF16), V((G, 2 * cap, 2 * M), BF16),
         V((G, 2 * cap, M), BF16), V((G, 2 * cap, 128), F32), V((G, 2 * cap, 128), F32),
@@ -644,27 +735,25 @@
         V((G, 2 * cap, C), BF16), V((G, 2 * cap, C), BF16), V((E, cap, C), BF16), V((E, cap, C), BF16),
         V((2, M, C), F32),
         V((G, M, C), BF16), V((G, M, C), F32), V((G, M, C), BF16), V((G, M, C), BF16), V((G, M, C), BF16),
-        V((M, C), BF16),
-        DMA((8,)), DMA((1,)), DMA((1,)), DMA((chunks,)),
-        DMA((1,)), DMA((G,)), DMA((1,)), DMA((1,)), DMA((1,)), DMA((1,)), DMA((1,)), DMA((chunks,)),
-        DMA((1,)), DMA((1,)), DMA((1,)), DMA((1,)), DMA((1,)), DMA((1,)),
+        V((G, M, C), BF16), V((M, C), BF16),
+        DMA((8,)), DMA((12,)), DMA((1,)), DMA((1,)), DMA((chunks,)),
+        DMA((1,)), DMA((G,)), DMA((1,)), DMA((1,)), DMA((1,)), DMA((1,)), DMA((1,)), DMA((chunks,)), DMA((chunks,)),
+        DMA((1,)), DMA((1,)), DMA((1,)), DMA((1,)), DMA((1,)), DMA((1,)), DMA((1,)), DMA((1,)),
         DMA((1,)), DMA((4, G)), DMA((G,)), DMA((1,)), DMA((G,)), DMA((G,)),
         DMA((1,)), DMA((2,)), DMA((1,)), DMA((G,)), DMA((1,)), DMA((1,)),
-        DMA((1,)), DMA((G,)), DMA((1,)), DMA((1,)),
+        DMA((1,)), DMA((G,)), DMA((1,)), DMA((1,)), DMA((1,)), DMA((1,)),
     ]
     outs = pl.pallas_call(
         functools.partial(layer_kernel, E, T, cap),
         out_shape=(V((M, C), BF16), V((M, C), F32), V((conv_state.shape[1], M, C), BF16)),
-        in_specs=[vm] * 12 + [anyspace] * 9,
+        in_specs=[anyspace] * 21,
         out_specs=(vm, vm, vm),
         scratch_shapes=scratch,
         compiler_params=pltpu.CompilerParams(
             collective_id=0, has_side_effects=True, vmem_limit_bytes=60 * 1024 * 1024
         ),
     )(
-        hidden, mix_gain, routes.T, route_weights.T, conv_state.transpose(1, 0, 2), conv_taps,
-        input_gate, decay_gate, decay_param[None, :], lru_state,
-        ffn_gain, branch_gate[None, :],
+        *small,
         proj_x, proj_y, dense_gate, dense_up, proj_out, expert_gate[0], expert_up[0], expert_down[0], dd,
     )
     new_hidden, new_lru, new_conv = pl.pallas_call(

time: 71.6 us -> 66.9 us (0.934)
  Pallas kernels: 70.8 us -> 66.1 us
    pallas_call x1, Pallas kernels: 70.1 us -> 65.3 us  [on_device(): pl.pallas_call(functools.partial(layer_kernel, E, T, cap), out_shape=(V((...]
where the time goes in v3:
time: 66.9 us; the launch traced here: 66.7 us
  Pallas kernels  66.1 us (99%)
    pallas_call x1, Pallas kernels, on_device(): pl.pallas_call(functools.partial(layer_kernel, E, T, cap), out_shape=(V((...  65.3 us

profile of v3, /device:TPU:0, one launch (start us, length us, event | category | flops | bytes accessed | tf_op | source)
XLA Modules:
  0.0 66.7 jit_solution(9854748908814357889)
XLA Ops:
  0.6 65.3 %shard_map.220 = (bf16[64,512]{1,0:T(8,128)(2,1)S(1)}, f32[64,512]{1,0:T(8,128)S(1)}, bf16[3,64,512]{2,1,0:T(8,128)(2,1)S(1)}) custom-call(bf16[64,2048]{1,0:T(8,128)(2,1)} %hidden_h.1, bf16[2048]{0:T(1024)(128)(2,1)} %mix_gain_h.1, s32[2,64]{1,0:T(2,128)} %bitcast.17, f32[2,64]{1,0:T(2,128)} %bitcast.18, bf16[3,64,512]{2,1,0:T(8,128)(2,1)} %bitcast.14, ...), custom_call_target="tpu_custom_call" | custom-call | tf_op jit(solution)/shard_map/pallas_call | solution.py:746
  65.9 0.8 %shard_map.221 = (bf16[64,512]{1,0:T(8,128)(2,1)}, f32[64,512]{1,0:T(8,128)}, bf16[3,64,512]{2,1,0:T(8,128)(2,1)}) custom-call(bf16[64,512]{1,0:T(8,128)(2,1)S(1)} %get-tuple-element.9.a, f32[64,512]{1,0:T(8,128)S(1)} %get-tuple-element.10.b, bf16[3,64,512]{2,1,0:T(8,128)(2,1)S(1)} %get-tuple-element.11.c), custom_call_target="tpu_custom_call" | custom-call | tf_op jit(solution)/shard_map/pallas_call | solution.py:759

commit v4 on v3

--- a/solution.py
+++ b/solution.py
@@ -197,6 +197,52 @@
         nb_in(g).wait_recv()
         nb_beside(g).start()
 
+    early = max(0, chunks - DIRECT) if paired else 0
+    last = flip(g0, upper)
+
+    def z_copy(i, g):
+        return rcopy(zout.at[i, g], zrec.at[i, g0], pz_s.at[0], pz_r.at[i], ep=2 * g + par)
+
+    def z_in(i):
+        some = pl.ds(0, upper if i < early else G - 1)
+        return rcopy(zout.at[i, some], zrec.at[i, some], pz_s.at[0], pz_r.at[i], ep=mate)
+
+    def z_pair(i):
+        some = pl.ds(0, upper - 1)
+        rcopy(zout.at[i, some], zpair.at[i, some], pz_s.at[0], zx_r.at[i], ep=mate).wait_recv()
+        total = zlast[i]
+        for low in range(1, upper):
+            total = total + zpair[i, flip(g0, low)].astype(F32)
+        zout[i, last] = total.astype(BF16)
+        z_copy(i, last).start()
+
+    nb_all = rcopy(xin.at[rest, core], xin.at[rest, core], nf_s.at[0], nf_r.at[0], tp=beside)
+    nb_all.wait_recv()
+    for i in range(chunks):
+        w_in(i).wait_recv()
+        z = dot(xin[...].reshape(G * M, 2 * R), wall[i].reshape(2 * R, CW)).reshape(G, M, CW)
+        zf[...] = z
+        zout[i] = z.astype(BF16)
+
+        if i < early:
+            for low in range(1, upper):
+                to = flip(g0, low)
+                g = flip(to, upper)
+                rcopy(zout.at[i, g], zpair.at[i, g0], pz_s.at[0], zx_r.at[i], ep=2 * to + par).start()
+                z_copy(i, to).start()
+            zlast[i] = zf[last]
+        else:
+            @pl.loop(1, G)
+            def _(k):
+                z_copy(i, peer_group(k)).start()
+
+        acc[:, i * CW:(i + 1) * CW] = zf[g0]
+        if 0 <= i - 2 < early:
+            z_pair(i - 2)
+
+    for i in range(max(0, chunks - 2), early):
+        z_pair(i)
+
     others = pl.ds(0, E - 1)
     ct_all = rcopy(ct.at[others], ctr.at[others], ct_s.at[0], ct_r.at[0], ep=mate)
     ct_all.wait_recv()
@@ -245,52 +291,6 @@
     @pl.loop(0, G)
     def _(g):
         own_sel[g] = jnp.concatenate([own_hit(2 * g), own_hit(2 * g + 1)], axis=0).astype(BF16)
-
-    early = max(0, chunks - DIRECT) if paired else 0
-    last = flip(g0, upper)
-
-    def z_copy(i, g):
-        return rcopy(zout.at[i, g], zrec.at[i, g0], pz_s.at[0], pz_r.at[i], ep=2 * g + par)
-
-    def z_in(i):
-        some = pl.ds(0, upper if i < early else G - 1)
-        return rcopy(zout.at[i, some], zrec.at[i, some], pz_s.at[0], pz_r.at[i], ep=mate)
-
-    def z_pair(i):
-        some = pl.ds(0, upper - 1)
-        rcopy(zout.at[i, some], zpair.at[i, some], pz_s.at[0], zx_r.at[i], ep=mate).wait_recv()
-        total = zlast[i]
-        for low in range(1, upper):
-            total = total + zpair[i, flip(g0, low)].astype(F32)
-        zout[i, last] = total.astype(BF16)
-        z_copy(i, last).start()
-
-    nb_all = rcopy(xin.at[rest, core], xin.at[rest, core], nf_s.at[0], nf_r.at[0], tp=beside)
-    nb_all.wait_recv()
-    for i in range(chunks):
-        w_in(i).wait_recv()
-        z = dot(xin[...].reshape(G * M, 2 * R), wall[i].reshape(2 * R, CW)).reshape(G, M, CW)
-        zf[...] = z
-        zout[i] = z.astype(BF16)
-
-        if i < early:
-            for low in range(1, upper):
-                to = flip(g0, low)
-                g = flip(to, upper)
-                rcopy(zout.at[i, g], zpair.at[i, g0], pz_s.at[0], zx_r.at[i], ep=2 * to + par).start()
-                z_copy(i, to).start()
-            zlast[i] = zf[last]
-        else:
-            @pl.loop(1, G)
-            def _(k):
-                z_copy(i, peer_group(k)).start()
-
-        acc[:, i * CW:(i + 1) * CW] = zf[g0]
-        if 0 <= i - 2 < early:
-            z_pair(i - 2)
-
-    for i in range(max(0, chunks - 2), early):
-        z_pair(i)
 
     for i in range(chunks):
         z_in(i).wait_recv()

time: 66.9 us -> 66.9 us (level)
  no operation moved by 1% of the time
where the time goes in v4:
time: 66.9 us; the launch traced here: 66.7 us
  Pallas kernels  66.1 us (99%)
    pallas_call x1, Pallas kernels, on_device(): pl.pallas_call(functools.partial(layer_kernel, E, T, cap), out_shape=(V((...  65.3 us

profile of v4, /device:TPU:0, one launch (start us, length us, event | category | flops | bytes accessed | tf_op | source)
XLA Modules:
  0.0 66.7 jit_solution(5690256699010109721)
XLA Ops:
  0.6 65.3 %shard_map.220 = (bf16[64,512]{1,0:T(8,128)(2,1)S(1)}, f32[64,512]{1,0:T(8,128)S(1)}, bf16[3,64,512]{2,1,0:T(8,128)(2,1)S(1)}) custom-call(bf16[64,2048]{1,0:T(8,128)(2,1)} %hidden_h.1, bf16[2048]{0:T(1024)(128)(2,1)} %mix_gain_h.1, s32[2,64]{1,0:T(2,128)} %bitcast.17, f32[2,64]{1,0:T(2,128)} %bitcast.18, bf16[3,64,512]{2,1,0:T(8,128)(2,1)} %bitcast.14, ...), custom_call_target="tpu_custom_call" | custom-call | tf_op jit(solution)/shard_map/pallas_call | solution.py:746
  65.9 0.8 %shard_map.221 = (bf16[64,512]{1,0:T(8,128)(2,1)}, f32[64,512]{1,0:T(8,128)}, bf16[3,64,512]{2,1,0:T(8,128)(2,1)}) custom-call(bf16[64,512]{1,0:T(8,128)(2,1)S(1)} %get-tuple-element.9.a, f32[64,512]{1,0:T(8,128)S(1)} %get-tuple-element.10.b, bf16[3,64,512]{2,1,0:T(8,128)(2,1)S(1)} %get-tuple-element.11.c), custom_call_target="tpu_custom_call" | custom-call | tf_op jit(solution)/shard_map/pallas_call | solution.py:759
